TPU v7x, 32 devices: a whole 2x2x4 slice. The times are simulated.
32 devices in a mesh: sp: 8 (over z, y), tp: 4 (over x, core).
Axes of the slice: x: 2, y: 2, z: 4, core: 2. Of those that a mesh axis runs over, the one named last changes fastest.
Arguments:
- queries_one: bfloat16 [2048, 512], P('sp', 'tp'), may hold values from -6 to 6
- queries_two: bfloat16 [2048, 512], P('sp', 'tp'), may hold values from -6 to 6
- keys_one: bfloat16 [2048, 512], P('sp', 'tp'), may hold values from -6 to 6
- keys_two: bfloat16 [2048, 512], P('sp', 'tp'), may hold values from -6 to 6
- values: bfloat16 [2048, 1024], P('sp', 'tp'), may hold values from -6 to 6
- mix_lambda: float32 [4], P('tp'), may hold values from 0.3 to 0.8
- head_gain: float32 [1024], P('tp'), may hold values from 0.1 to 1.9
- out_weight: bfloat16 [1024, 2048], P('tp'), may hold values from -0.1875 to 0.1875
- residual_in: bfloat16 [2048, 2048], P('sp', 'tp'), may hold values from -12 to 12
- norm_gain: float32 [2048], replicated, may hold values from 0.1 to 1.9
- gate_weight: bfloat16 [2048, 5632], P('sp', 'tp'), may hold values from -0.125 to 0.125
- up_weight: bfloat16 [2048, 5632], P('sp', 'tp'), may hold values from -0.125 to 0.125
- down_weight: bfloat16 [5632, 2048], P('tp', 'sp'), may hold values from -0.078125 to 0.078125
Outputs:
- layer_out: bfloat16 [2048, 2048], P('sp', 'tp')
All inputs are finite; a program needn't handle non-finite values.
Results may differ from a plain program's by a relative error of at most 0.012.
Values may be sent and summed in bfloat16 or wider, within the bound.
A program may use at most 192 MiB of HBM per device.

v0:
```python
import jax
import jax.numpy as jnp
from jax import lax
from jax.sharding import PartitionSpec as P

HEAD = 128


epsilon = 1e-06
masked_score = -1e30


def per_device(
    queries_one,
    queries_two,
    keys_one,
    keys_two,
    values,
    mix_lambda,
    head_gain,
    out_weight,
    residual_in,
    norm_gain,
    gate_weight,
    up_weight,
    down_weight,
):
    tok_rows = queries_one.shape[0]
    heads_here = mix_lambda.shape[0]
    head_width = HEAD
    value_width = values.shape[1] // heads_here
    query_pos = lax.axis_index("sp") * tok_rows + jnp.arange(tok_rows, dtype=jnp.int32)
    query_first = queries_one.reshape(tok_rows, heads_here, head_width)
    query_second = queries_two.reshape(tok_rows, heads_here, head_width)
    score_scale = head_width ** (-0.5)

    def update(state, queries, key_rows, value_rows, visible):
        running, totals, weighted = state
        scores = (
            jnp.einsum("qhd,khd->hqk", queries, key_rows, preferred_element_type=jnp.float32)
            * score_scale
        )
        scores = jnp.where(visible[None], scores, masked_score)
        highest = jnp.maximum(running, jnp.max(scores, axis=2))
        weights_exp = jnp.where(visible[None], jnp.exp(scores - highest[..., None]), 0.0)
        totals = jnp.sum(weights_exp, axis=2)
        weighted = jnp.einsum(
            "hqk,khd->hqd",
            weights_exp.astype(jnp.bfloat16),
            value_rows,
            preferred_element_type=jnp.float32,
        )
        return (highest, totals, weighted)

    initial = (
        jnp.full((heads_here, tok_rows), masked_score, jnp.float32),
        jnp.zeros((heads_here, tok_rows), jnp.float32),
        jnp.zeros((heads_here, tok_rows, value_width), jnp.float32),
    )
    key_first = lax.all_gather(keys_one, "sp", axis=0, tiled=True)
    key_second = lax.all_gather(keys_two, "sp", axis=0, tiled=True)
    value_piece = lax.all_gather(values, "sp", axis=0, tiled=True)
    key_count = key_first.shape[0]
    key_pos = jnp.arange(key_count, dtype=jnp.int32)
    visible = key_pos[None, :] <= query_pos[:, None]
    value_rows = value_piece.reshape(key_count, heads_here, value_width)
    first_new = update(
        initial,
        query_first,
        key_first.reshape(key_count, heads_here, head_width),
        value_rows,
        visible,
    )
    second_new = update(
        initial,
        query_second,
        key_second.reshape(key_count, heads_here, head_width),
        value_rows,
        visible,
    )
    lam_heads = mix_lambda[:, None, None]
    mixed = (
        first_new[2] / first_new[1][..., None]
        - lam_heads * second_new[2] / second_new[1][..., None]
    )
    mean_square = jnp.mean(mixed * mixed, axis=2, keepdims=True)
    normed_heads = (
        mixed
        * lax.rsqrt(mean_square + epsilon)
        * head_gain.reshape(heads_here, 1, value_width)
        * 0.8
    )
    attended = (
        normed_heads.transpose(1, 0, 2)
        .reshape(tok_rows, heads_here * value_width)
        .astype(jnp.bfloat16)
    )
    projected = lax.psum_scatter(
        lax.dot_general(
            out_weight, attended, (((0,), (1,)), ((), ())), preferred_element_type=jnp.float32
        ).astype(jnp.bfloat16),
        "tp",
        scatter_dimension=0,
        tiled=True,
    ).astype(jnp.float32)
    resid = (residual_in.astype(jnp.float32) + projected.T).astype(jnp.bfloat16)
    full_rows = lax.all_gather(resid, "tp", axis=1, tiled=True)
    full_float = full_rows.astype(jnp.float32)
    mean_rows = jnp.mean(full_float * full_float, axis=1, keepdims=True)
    normed = (full_float * lax.rsqrt(mean_rows + epsilon) * norm_gain[None, :]).astype(jnp.bfloat16)
    gate_act = jnp.dot(
        normed,
        lax.all_gather(gate_weight, "sp", axis=0, tiled=True),
        preferred_element_type=jnp.float32,
    )
    up_act = jnp.dot(
        normed,
        lax.all_gather(up_weight, "sp", axis=0, tiled=True),
        preferred_element_type=jnp.float32,
    )
    hidden = (jax.nn.silu(gate_act) * up_act).astype(jnp.bfloat16)
    partials = jnp.dot(
        hidden,
        lax.all_gather(down_weight, "sp", axis=1, tiled=True),
        preferred_element_type=jnp.float32,
    )
    mlp_out = lax.psum_scatter(
        partials.astype(jnp.bfloat16), "tp", scatter_dimension=1, tiled=True
    ).astype(jnp.float32)
    return (resid.astype(jnp.float32) + mlp_out).astype(jnp.bfloat16)


def solution(mesh):
    in_specs = (
        P("sp", "tp"),
        P("sp", "tp"),
        P("sp", "tp"),
        P("sp", "tp"),
        P("sp", "tp"),
        P("tp"),
        P("tp"),
        P("tp", None),
        P("sp", "tp"),
        P(),
        P("sp", "tp"),
        P("sp", "tp"),
        P("tp", "sp"),
    )
    out_specs = P("sp", "tp")
    return jax.shard_map(
        per_device, mesh=mesh, in_specs=in_specs, out_specs=out_specs, check_vma=False
    )
```

profile of v0, /device:TPU:13, one launch (start us, length us, event | category | flops | bytes accessed | tf_op | source)
XLA Modules:
  0.0 447.4 jit_solution(3199958501547778345)
XLA Ops:
  6.5 0.0 copy-start
  6.5 0.0 all-gather.6.cloned.1.call-start
  6.5 0.7 all-gather.6.cloned.1.call-update
  7.3 0.0 reduce-scatter.3.cloned.1.call-start
  8.0 23.9 %all_gather.23 = bf16[2048,128]{1,0:T(8,128)(2,1)S(1)} all-gather(bf16[256,128]{1,0:T(8,128)(2,1)} %param.16), channel_id=1, replica_groups=mesh['sp'=8,'tp'=4] {'sp'}, dimensions={0}, use_global_device_ids=true | all-gather | bytes 589824 | tf_op jit(solution)/shard_map/all_gather | solution.py:61
  31.8 1.4 fusion.34
  33.3 0.0 copy-done.5
  33.3 26.1 %all_gather.21 = bf16[2048,128]{1,0:T(8,128)(2,1)S(1)} all-gather(bf16[256,128]{1,0:T(8,128)(2,1)S(1)} %copy-done.5), channel_id=1, replica_groups=mesh['sp'=8,'tp'=4] {'sp'}, dimensions={0}, use_global_device_ids=true | all-gather | bytes 589824 | tf_op jit(solution)/shard_map/all_gather | solution.py:60
  59.4 0.0 copy-done.8
  59.4 0.6 fusion.33
  60.0 1.3 copy-done.2
  61.3 1.2 fusion.9
  62.5 0.0 all-gather.6.cloned.1.call-done
  62.5 0.0 copy-start.7
  62.5 2.7 convolution_divide_fusion
  65.2 0.0 copy-done.7
  65.3 0.0 copy-start.6
  65.3 0.8 multiply_reduce_fusion
  66.1 0.0 copy-start.4
  66.1 0.0 copy-done
  66.1 0.0 copy-done.6
  66.1 1.5 fusion.3
  67.6 0.0 reduce-scatter.3.cloned.1.call-update
  67.7 0.0 copy-start.9
  67.7 0.0 all-gather.8.cloned.1.call-start
  67.7 39.9 %reduce-scatter.3.cloned.1.call-done = bf16[512,256]{0,1:T(8,128)(2,1)} async-done(((bf16[2048,256]{0,1:T(8,128)(2,1)}), bf16[512,256]{0,1:T(8,128)(2,1)}) %reduce-scatter.3.cloned.1.call-update) | async-done | bytes 262160 | tf_op jit(solution)/shard_map/reduce_scatter | solution.py:98
  107.6 0.0 copy-done.4
  107.6 1.7 fusion.21
  109.3 0.0 all-gather.8.cloned.1.call-update
  109.3 0.0 all-gather.10.cloned.1.call-start
  109.4 0.5 all-gather.10.cloned.1.call-update
  109.9 0.0 all-gather.12.cloned.1.call-start
  110.0 0.5 all-gather.12.cloned.1.call-update
  110.5 0.0 all-gather.14.cloned.1.call-start
  110.5 0.5 all-gather.14.cloned.1.call-update
  111.1 0.0 reduce-scatter.5.cloned.1.call-start
  111.1 15.6 %all-gather.8.cloned.1.call-done = bf16[256,2048]{1,0:T(8,128)(2,1)} async-done(((bf16[256,512]{1,0:T(8,128)(2,1)}), bf16[256,2048]{1,0:T(8,128)(2,1)}) %all-gather.8.cloned.1.call-update) | async-done | bytes 1048592 | tf_op jit(solution)/shard_map/all_gather | solution.py:107
  126.8 1.5 fusion.4
  128.3 0.0 copy-start.3
  128.3 89.1 %all-gather.10.cloned.1.call-done = bf16[2048,1408]{1,0:T(8,128)(2,1)} async-done(((bf16[256,1408]{1,0:T(8,128)(2,1)}), bf16[2048,1408]{1,0:T(8,128)(2,1)}) %all-gather.10.cloned.1.call-update) | async-done | bytes 5767184 | tf_op jit(solution)/shard_map/all_gather | solution.py:113
  217.4 6.0 %fusion.24 = f32[256,1408]{1,0:T(8,128)} fusion(bf16[2048,1408]{1,0:T(8,128)(2,1)} %all-gather.10.cloned.1.call-done, bf16[256,2048]{1,0:T(8,128)(2,1)} %all-gather.8.cloned.1.call-done, f32[2048]{0:T(1024)S(1)} %copy-done.9, f32[256]{0:T(256)S(1)} %add_rsqrt_fusion), kind=kOutput, calls=%fused_computation.34 | convolution fusion | flops 1478492160 | bytes 8266752 | tf_op jit(solution)/shard_map/dot_general | solution.py:111
  223.4 86.6 %all-gather.12.cloned.1.call-done = bf16[2048,1408]{1,0:T(8,128)(2,1)} async-done(((bf16[256,1408]{1,0:T(8,128)(2,1)}), bf16[2048,1408]{1,0:T(8,128)(2,1)}) %all-gather.12.cloned.1.call-update) | async-done | bytes 5767184 | tf_op jit(solution)/shard_map/all_gather | solution.py:118
  310.0 93.3 %all-gather.14.cloned.1.call-done = bf16[1408,2048]{1,0:T(8,128)(2,1)} async-done(((bf16[1408,256]{1,0:T(8,128)(2,1)}), bf16[1408,2048]{1,0:T(8,128)(2,1)}) %all-gather.14.cloned.1.call-update) | async-done | bytes 5767184 | tf_op jit(solution)/shard_map/all_gather | solution.py:124
  403.3 0.0 copy-done.3
  403.3 9.3 %convolution_convert_fusion.1 = bf16[256,2048]{1,0:T(8,128)(2,1)} fusion(bf16[1408,2048]{1,0:T(8,128)(2,1)} %all-gather.14.cloned.1.call-done, bf16[2048,1408]{1,0:T(8,128)(2,1)} %all-gather.12.cloned.1.call-done, f32[256,1408]{1,0:T(8,128)} %fusion.24, bf16[256,2048]{1,0:T(8,128)(2,1)S(1)} %copy-done.3, f32[2048]{0:T(1024)S(1)} %copy-done.9, ...), kind=kOutput, calls=%fused_computation.9 | convolution fusion | flops 2957574144 | bytes 15082496 | tf_op jit(solution)/shard_map/dot_general | solution.py:122
  412.5 0.0 reduce-scatter.5.cloned.1.call-update
  412.6 26.2 %reduce-scatter.5.cloned.1.call-done = bf16[256,512]{1,0:T(8,128)(2,1)} async-done(((bf16[256,2048]{1,0:T(8,128)(2,1)}), bf16[256,512]{1,0:T(8,128)(2,1)}) %reduce-scatter.5.cloned.1.call-update) | async-done | bytes 262160 | tf_op jit(solution)/shard_map/reduce_scatter | solution.py:127
  438.8 1.7 add_convert_fusion
  (11 shorter events, 0.0 us)
Async XLA Ops:
  6.5 59.6 %copy-start = (bf16[256,2048]{1,0:T(8,128)(2,1)S(1)}, bf16[256,2048]{1,0:T(8,128)(2,1)}, u32[]{:S(2)}) copy-start(bf16[256,2048]{1,0:T(8,128)(2,1)} %param.20) | copy-start | bytes 3145732
  6.5 26.7 %copy-start.5 = (bf16[256,128]{1,0:T(8,128)(2,1)S(1)}, bf16[256,128]{1,0:T(8,128)(2,1)}, u32[]{:S(2)}) copy-start(bf16[256,128]{1,0:T(8,128)(2,1)} %param.15) | copy-start | bytes 196612
  6.5 52.8 %copy-start.8 = (bf16[256,128]{1,0:T(8,128)(2,1)S(1)}, bf16[256,128]{1,0:T(8,128)(2,1)}, u32[]{:S(2)}) copy-start(bf16[256,128]{1,0:T(8,128)(2,1)} %param.13) | copy-start | bytes 196612
  6.5 56.0 %all-gather.6.cloned.1.call-start = ((), (), s32[]{:S(2)}) async-start(), calls=%async_computation.2 | async-start | bytes 1179648 | tf_op jit(solution)/shard_map/all_gather | solution.py:62
  7.3 100.3 %reduce-scatter.3.cloned.1.call-start = ((), (), s32[]{:S(2)}) async-start(), calls=%async_computation.3 | async-start | bytes 1310720 | tf_op jit(solution)/shard_map/reduce_scatter | solution.py:98
  60.0 1.3 copy-start.2
  62.5 2.7 copy-start.7
  65.3 0.9 copy-start.6
  66.1 41.5 %copy-start.4 = (bf16[256,512]{1,0:T(8,128)(2,1)S(1)}, bf16[256,512]{1,0:T(8,128)(2,1)}, u32[]{:S(2)}) copy-start(bf16[256,512]{1,0:T(8,128)(2,1)} %param.21) | copy-start | bytes 786436
  67.7 149.8 %copy-start.9 = (f32[2048]{0:T(1024)S(1)}, f32[2048]{0:T(1024)}, u32[]{:S(2)}) copy-start(f32[2048]{0:T(1024)} %param.22) | copy-start | bytes 24580
  67.7 59.1 %all-gather.8.cloned.1.call-start = ((), (), s32[]{:S(2)}) async-start(), calls=%async_computation.4 | async-start | bytes 1310720 | tf_op jit(solution)/shard_map/all_gather | solution.py:107
  109.3 108.1 %all-gather.10.cloned.1.call-start = ((), (), s32[]{:S(2)}) async-start(), calls=%async_computation.5 | async-start | bytes 6488064 | tf_op jit(solution)/shard_map/all_gather | solution.py:113
  109.9 200.1 %all-gather.12.cloned.1.call-start = ((), (), s32[]{:S(2)}) async-start(), calls=%async_computation.6 | async-start | bytes 6488064 | tf_op jit(solution)/shard_map/all_gather | solution.py:118
  110.5 292.8 %all-gather.14.cloned.1.call-start = ((), (), s32[]{:S(2)}) async-start(), calls=%async_computation.7 | async-start | bytes 6488064 | tf_op jit(solution)/shard_map/all_gather | solution.py:124
  111.1 327.7 %reduce-scatter.5.cloned.1.call-start = ((), (), s32[]{:S(2)}) async-start(), calls=%async_computation.8 | async-start | bytes 1310720 | tf_op jit(solution)/shard_map/reduce_scatter | solution.py:127
  128.3 275.0 %copy-start.3 = (bf16[256,2048]{1,0:T(8,128)(2,1)S(1)}, bf16[256,2048]{1,0:T(8,128)(2,1)}, u32[]{:S(2)}) copy-start(bf16[256,2048]{1,0:T(8,128)(2,1)} %all-gather.8.cloned.1.call-done) | copy-start | bytes 3145732
  223.4 215.4 %copy-start.1 = (bf16[256,512]{1,0:T(8,128)(2,1)S(1)}, bf16[256,512]{1,0:T(8,128)(2,1)}, u32[]{:S(2)}) copy-start(bf16[256,512]{1,0:T(8,128)(2,1)} %fusion.21) | copy-start | bytes 786436
Sparse Core Ops, SparseCore 0:
  9.5 41.1 all-gather.5
  67.8 39.7 reduce-scatter.2
  109.5 17.2 all-gather.7
  128.8 88.5 all-gather.9
  219.4 90.4 all-gather.11
  311.9 91.3 all-gather.13
  412.7 26.0 reduce-scatter.4
where the time goes:
time: 449 us; the launch traced here: 447 us
  waiting for transfers between devices  353 us (79%)
  blocking collectives  50 us (11%)
  matrix products  22.3 us (5%)
  between operations  14.3 us (3%)
  other arithmetic  6.13 us (1%)
    all_gather x1, waiting for transfers between devices, per_device(): lax.all_gather(down_weight, 'sp', axis=1, tiled=True)  93.3 us
    all_gather x1, waiting for transfers between devices, per_device(): lax.all_gather(gate_weight, 'sp', axis=0, tiled=True)  89.1 us
    all_gather x1, waiting for transfers between devices, per_device(): lax.all_gather(up_weight, 'sp', axis=0, tiled=True)  86.6 us
    reduce_scatter x1, waiting for transfers between devices, per_device(): lax.psum_scatter(lax.dot_general(out_weight, attended, (((0,), (1,)), (()...  39.9 us
    reduce_scatter x1, waiting for transfers between devices, per_device(): lax.psum_scatter(partials.astype(jnp.bfloat16), 'tp', scatter_dimension=1...  26.2 us
    all_gather x1, blocking collectives, per_device(): key_first = lax.all_gather(keys_one, 'sp', axis=0, tiled=True)  26.1 us
    all_gather x1, blocking collectives, per_device(): key_second = lax.all_gather(keys_two, 'sp', axis=0, tiled=True)  23.9 us
    all_gather x1, waiting for transfers between devices, per_device(): full_rows = lax.all_gather(resid, 'tp', axis=1, tiled=True)  15.6 us
  transfers between devices with their start and end apart: 7, of which 6 were waited for; matrix products, arithmetic and copies ran while one was open for 2% of the time, Pallas kernels for 0%

commit v1 on v0

--- a/solution.py
+++ b/solution.py
@@ -1,6 +1,10 @@
+import functools
+
 import jax
 import jax.numpy as jnp
 from jax import lax
+from jax.experimental import pallas as pl
+from jax.experimental.pallas import tpu as pltpu
 from jax.sharding import PartitionSpec as P
 
 HEAD = 128
@@ -130,6 +134,374 @@
     return (resid.astype(jnp.float32) + mlp_out).astype(jnp.bfloat16)
 
 
+def remote(src, dst, send, recv, where):
+    return pltpu.make_async_remote_copy(
+        src_ref=src,
+        dst_ref=dst,
+        send_sem=send,
+        recv_sem=recv,
+        device_id=where,
+        device_id_type=pl.DeviceIdType.MESH,
+    )
+
+
+def greet(peers):
+    barrier = pltpu.get_barrier_semaphore()
+    for where in peers:
+        pl.semaphore_signal(
+            barrier, inc=1, device_id=where, device_id_type=pl.DeviceIdType.MESH
+        )
+    pl.semaphore_wait(barrier, len(peers))
+
+
+def neighbours(n_sp, n_tp):
+    s, t = lax.axis_index("sp"), lax.axis_index("tp")
+    y_peer = s + 1 - 2 * lax.rem(s, 2)
+    sibling = t + 1 - 2 * lax.rem(t, 2)
+    across = lax.rem(t + 2, n_tp)
+    return s, t, y_peer, sibling, across
+
+
+def spread_kernel(n_sp, n_tp, w_ref, kv_ref, wall, kvall, *sems):
+    kv_s, kv_r, a_s, a_r, x_s, x_r, c_s, c_r, f_s, f_r, loc = sems
+    s, t, _, sibling, across = neighbours(n_sp, n_tp)
+    rows = kv_ref.shape[0]
+    part = w_ref.shape[1] // n_sp
+    depth = w_ref.shape[2]
+    greet(
+        [{"sp": lax.rem(s + i, n_sp)} for i in range(1, n_sp)]
+        + [{"tp": sibling}, {"tp": across}]
+    )
+
+    def block(who, source):
+        return wall.at[:, who, :, pl.ds(pl.multiple_of(source * depth, depth), depth)]
+
+    def piece(dest):
+        return w_ref.at[:, pl.ds(pl.multiple_of(dest * part, 16), part), :]
+
+    pending = []
+    kv_in, a_in = [], []
+    mine = kvall.at[pl.ds(pl.multiple_of(s * rows, rows), rows), :]
+    for i in range(1, n_sp):
+        copy = remote(kv_ref, mine, kv_s.at[i - 1], kv_r.at[i - 1], {"sp": lax.rem(s + i, n_sp)})
+        copy.start()
+        kv_in.append(copy)
+    for i in range(1, n_sp):
+        p = lax.rem(s + i, n_sp)
+        copy = remote(piece(p), block(t, s), a_s.at[i - 1], a_r.at[i - 1], {"sp": p})
+        copy.start()
+        a_in.append(copy)
+    own_kv = pltpu.make_async_copy(kv_ref, mine, loc.at[0])
+    own_kv.start()
+    own_w = pltpu.make_async_copy(piece(s), block(t, s), loc.at[1])
+    own_w.start()
+    x_in, c_in, f_in = [], [], []
+
+    def forward(i):
+        source = lax.rem(s - i + n_sp, n_sp)
+        remote(
+            block(t, source), block(t, source), x_s.at[i], x_r.at[i], {"tp": across}
+        ).wait_recv()
+        copy = remote(
+            block(across, source), block(across, source), f_s.at[i], f_r.at[i], {"tp": sibling}
+        )
+        copy.start()
+        f_in.append(copy)
+
+    for i in range(n_sp):
+        source = lax.rem(s - i + n_sp, n_sp)
+        if i == 0:
+            own_w.wait()
+        else:
+            a_in[i - 1].wait_recv()
+        for send, recv, where, into in ((x_s, x_r, across, x_in), (c_s, c_r, sibling, c_in)):
+            copy = remote(
+                block(t, source), block(t, source), send.at[i], recv.at[i], {"tp": where}
+            )
+            copy.start()
+            into.append(copy)
+        if i >= 1:
+            forward(i - 1)
+    forward(n_sp - 1)
+    own_kv.wait()
+    for copy in kv_in:
+        copy.wait()
+    for copy in a_in + x_in:
+        copy.wait_send()
+    for copy in c_in + f_in:
+        copy.wait()
+
+
+def spread(weights, kv, n_sp, n_tp):
+    three, ff_here, depth = weights.shape
+    dma = pltpu.SemaphoreType.DMA
+    return pl.pallas_call(
+        functools.partial(spread_kernel, n_sp, n_tp),
+        out_shape=(
+            jax.ShapeDtypeStruct((three, n_tp, ff_here // n_sp, depth * n_sp), weights.dtype),
+            jax.ShapeDtypeStruct((kv.shape[0] * n_sp, kv.shape[1]), kv.dtype),
+        ),
+        in_specs=[pl.BlockSpec(memory_space=pltpu.VMEM)] * 2,
+        out_specs=[pl.BlockSpec(memory_space=pltpu.VMEM)] * 2,
+        scratch_shapes=[dma((n_sp - 1,))] * 4 + [dma((n_sp,))] * 6 + [dma((2,))],
+        compiler_params=pltpu.CompilerParams(
+            collective_id=0, has_side_effects=True, vmem_limit_bytes=48 * 2**20
+        ),
+        name="spread",
+    )(weights, kv)
+
+
+def middle_kernel(
+    n_sp, n_tp, part_ref, res_ref, gain_ref, resid_ref, nall, pbuf, rbuf, nbuf,
+    p_s, p_r, q_s, q_r, z_s, z_r, y_s, y_r,
+):
+    s, t, y_peer, _, _ = neighbours(n_sp, n_tp)
+    half = n_sp // 2
+    rows = nbuf.shape[0]
+    cols = res_ref.shape[1]
+    greet(
+        [{"tp": lax.rem(t + j, n_tp)} for j in range(1, n_tp)]
+        + [{"sp": y_peer}]
+        + [{"sp": lax.rem(s + 2 * j, n_sp)} for j in range(1, half)]
+    )
+    sent = []
+
+    def take(p):
+        return pl.ds(pl.multiple_of(p * rows, rows), rows)
+
+    here = pl.ds(pl.multiple_of(t * cols, cols), cols)
+    for j in range(1, n_tp):
+        p = lax.rem(t + j, n_tp)
+        one = remote(part_ref.at[take(p), :], pbuf.at[j - 1], p_s.at[j - 1], p_r.at[j - 1], {"tp": p})
+        two = remote(
+            res_ref.at[take(p), :], rbuf.at[:, here], q_s.at[j - 1], q_r.at[j - 1], {"tp": p}
+        )
+        one.start()
+        two.start()
+        sent += [one, two]
+    rbuf[:, here] = res_ref[take(t), :]
+    total = part_ref[take(t), :].astype(jnp.float32)
+    for copy in sent:
+        copy.wait()
+    for j in range(1, n_tp):
+        total = total + pbuf[j - 1].astype(jnp.float32)
+    resid = (rbuf[...].astype(jnp.float32) + total).astype(jnp.bfloat16)
+    resid_ref[...] = resid
+    wide = resid.astype(jnp.float32)
+    mean = jnp.mean(wide * wide, axis=1, keepdims=True)
+    normed = (wide * lax.rsqrt(mean + epsilon) * gain_ref[...]).astype(jnp.bfloat16)
+    nbuf[...] = normed
+    z_in, y_in = [], []
+    for j in range(1, half):
+        copy = remote(
+            nbuf, nall.at[s], z_s.at[j - 1], z_r.at[j - 1], {"sp": lax.rem(s + 2 * j, n_sp)}
+        )
+        copy.start()
+        z_in.append(copy)
+    copy = remote(nbuf, nall.at[s], y_s.at[0], y_r.at[0], {"sp": y_peer})
+    copy.start()
+    y_in.append(copy)
+    nall[s] = normed
+    for j in range(1, half):
+        z_in[j - 1].wait_recv()
+        source = lax.rem(s - 2 * j + n_sp, n_sp)
+        copy = remote(nall.at[source], nall.at[source], y_s.at[j], y_r.at[j], {"sp": y_peer})
+        copy.start()
+        y_in.append(copy)
+    for copy in z_in:
+        copy.wait_send()
+    for copy in y_in:
+        copy.wait()
+
+
+def middle(part, residual, gain, n_sp, n_tp):
+    rows, width = part.shape[0] // n_tp, part.shape[1]
+    dma = pltpu.SemaphoreType.DMA
+    half = n_sp // 2
+    return pl.pallas_call(
+        functools.partial(middle_kernel, n_sp, n_tp),
+        out_shape=(
+            jax.ShapeDtypeStruct((rows, width), jnp.bfloat16),
+            jax.ShapeDtypeStruct((n_sp, rows, width), jnp.bfloat16),
+        ),
+        in_specs=[pl.BlockSpec(memory_space=pltpu.VMEM)] * 3,
+        out_specs=[pl.BlockSpec(memory_space=pltpu.VMEM)] * 2,
+        scratch_shapes=[
+            pltpu.VMEM((n_tp - 1, rows, width), jnp.bfloat16),
+            pltpu.VMEM((rows, width), jnp.bfloat16),
+            pltpu.VMEM((rows, width), jnp.bfloat16),
+        ]
+        + [dma((n_tp - 1,))] * 4
+        + [dma((half - 1,))] * 2
+        + [dma((half,))] * 2,
+        compiler_params=pltpu.CompilerParams(collective_id=1, has_side_effects=True),
+        name="middle",
+    )(part, residual, gain)
+
+
+def finish_kernel(
+    n_sp, n_tp, part_ref, resid_ref, out_ref, ybuf, cbuf, zbuf, fbuf,
+    y_s, y_r, z_s, z_r, o_s, o_r,
+):
+    s, t, y_peer, _, _ = neighbours(n_sp, n_tp)
+    half = n_sp // 2
+    rows = fbuf.shape[0]
+    cols = out_ref.shape[1]
+    greet(
+        [{"tp": lax.rem(t + j, n_tp)} for j in range(1, n_tp)]
+        + [{"sp": y_peer}]
+        + [{"sp": lax.rem(s + 2 * j, n_sp)} for j in range(1, half)]
+    )
+    order = list(range(1, half)) + [0]
+    y_in = {}
+    for j in order:
+        copy = remote(
+            part_ref.at[lax.rem(y_peer + 2 * j, n_sp)], ybuf.at[j], y_s.at[j], y_r.at[j],
+            {"sp": y_peer},
+        )
+        copy.start()
+        y_in[j] = copy
+    z_in = []
+    for j in order:
+        y_in[j].wait_recv()
+        both = part_ref[lax.rem(s + 2 * j, n_sp)].astype(jnp.float32) + ybuf[j].astype(jnp.float32)
+        if j == 0:
+            total = both
+        else:
+            cbuf[j - 1] = both.astype(jnp.bfloat16)
+            copy = remote(
+                cbuf.at[j - 1], zbuf.at[j - 1], z_s.at[j - 1], z_r.at[j - 1],
+                {"sp": lax.rem(s + 2 * j, n_sp)},
+            )
+            copy.start()
+            z_in.append(copy)
+    for j in range(1, half):
+        z_in[j - 1].wait_recv()
+        total = total + zbuf[j - 1].astype(jnp.float32)
+    fbuf[...] = (resid_ref[...].astype(jnp.float32) + total).astype(jnp.bfloat16)
+    mine = pl.ds(pl.multiple_of(t * rows, rows), rows)
+    out = []
+    for j in range(1, n_tp):
+        p = lax.rem(t + j, n_tp)
+        copy = remote(
+            fbuf.at[:, pl.ds(pl.multiple_of(p * cols, cols), cols)], out_ref.at[mine, :],
+            o_s.at[j - 1], o_r.at[j - 1], {"tp": p},
+        )
+        copy.start()
+        out.append(copy)
+    out_ref[mine, :] = fbuf[:, pl.ds(pl.multiple_of(t * cols, cols), cols)]
+    for copy in out:
+        copy.wait()
+    for j in order:
+        y_in[j].wait_send()
+    for copy in z_in:
+        copy.wait_send()
+
+
+def finish(part, resid, n_sp, n_tp):
+    _, rows, width = part.shape
+    dma = pltpu.SemaphoreType.DMA
+    half = n_sp // 2
+    block = (rows, width)
+    return pl.pallas_call(
+        functools.partial(finish_kernel, n_sp, n_tp),
+        out_shape=jax.ShapeDtypeStruct((rows * n_tp, width // n_tp), jnp.bfloat16),
+        in_specs=[pl.BlockSpec(memory_space=pltpu.VMEM)] * 2,
+        out_specs=pl.BlockSpec(memory_space=pltpu.VMEM),
+        scratch_shapes=[
+            pltpu.VMEM((half,) + block, jnp.bfloat16),
+            pltpu.VMEM((half - 1,) + block, jnp.bfloat16),
+            pltpu.VMEM((half - 1,) + block, jnp.bfloat16),
+            pltpu.VMEM(block, jnp.bfloat16),
+        ]
+        + [dma((half,))] * 2
+        + [dma((half - 1,))] * 2
+        + [dma((n_tp - 1,))] * 2,
+        compiler_params=pltpu.CompilerParams(collective_id=2, has_side_effects=True),
+        name="finish",
+    )(part, resid)
+
+
+def last_dot(left, right):
+    return lax.dot_general(
+        left, right, (((1,), (1,)), ((), ())), preferred_element_type=jnp.float32
+    )
+
+
+def split_hidden(
+    n_sp,
+    n_tp,
+    queries_one,
+    queries_two,
+    keys_one,
+    keys_two,
+    values,
+    mix_lambda,
+    head_gain,
+    out_weight,
+    residual_in,
+    norm_gain,
+    gate_weight,
+    up_weight,
+    down_weight,
+):
+    tok_rows = queries_one.shape[0]
+    weights = jnp.stack([gate_weight.T, up_weight.T, down_weight])
+    kv = jnp.concatenate([keys_one, keys_two, values], axis=1)
+    wall, kvall = spread(weights, kv, n_sp, n_tp)
+    query_pos = lax.axis_index("sp") * tok_rows + jnp.arange(tok_rows, dtype=jnp.int32)
+    key_pos = jnp.arange(kvall.shape[0], dtype=jnp.int32)
+    visible = key_pos[None, :] <= query_pos[:, None]
+    value_rows = kvall[:, 2 * HEAD :]
+
+    def one_map(queries, key_rows):
+        scores = last_dot(queries, key_rows) * HEAD ** (-0.5)
+        scores = jnp.where(visible, scores, masked_score)
+        weights_exp = jnp.exp(scores - jnp.max(scores, axis=1, keepdims=True))
+        totals = jnp.sum(weights_exp, axis=1, keepdims=True)
+        return (
+            jnp.dot(
+                weights_exp.astype(jnp.bfloat16), value_rows, preferred_element_type=jnp.float32
+            )
+            / totals
+        )
+
+    mixed = one_map(queries_one, kvall[:, :HEAD]) - mix_lambda[0] * one_map(
+        queries_two, kvall[:, HEAD : 2 * HEAD]
+    )
+    mean_square = jnp.mean(mixed * mixed, axis=1, keepdims=True)
+    attended = (mixed * lax.rsqrt(mean_square + epsilon) * head_gain[None, :] * 0.8).astype(
+        jnp.bfloat16
+    )
+    projected = jnp.dot(attended, out_weight, preferred_element_type=jnp.float32).astype(
+        jnp.bfloat16
+    )
+    resid, nall = middle(projected, residual_in, norm_gain[None, :], n_sp, n_tp)
+    width = nall.shape[2]
+    normed = nall.reshape(-1, width)
+    stacked = wall.reshape(3, -1, width)
+    gate_act = last_dot(normed, stacked[0])
+    up_act = last_dot(normed, stacked[1])
+    hidden = (jax.nn.silu(gate_act) * up_act).astype(jnp.bfloat16)
+    partials = jnp.dot(hidden, stacked[2], preferred_element_type=jnp.float32).astype(jnp.bfloat16)
+    return finish(partials.reshape(nall.shape), resid, n_sp, n_tp)
+
+
+def fits(n_sp, n_tp, shapes):
+    tokens, ff, width, heads = shapes
+    part = ff // (n_sp * n_tp)
+    return (
+        n_tp == 4
+        and heads == n_tp
+        and n_sp % 2 == 0
+        and n_sp > 2
+        and part % 16 == 0
+        and width % (n_sp * 128) == 0
+        and tokens % (n_sp * n_tp * 16) == 0
+        and tokens * width <= 2**23
+    )
+
+
 def solution(mesh):
     in_specs = (
         P("sp", "tp"),
@@ -147,6 +519,15 @@
         P("tp", "sp"),
     )
     out_specs = P("sp", "tp")
-    return jax.shard_map(
-        per_device, mesh=mesh, in_specs=in_specs, out_specs=out_specs, check_vma=False
-    )
+    n_sp, n_tp = mesh.shape["sp"], mesh.shape["tp"]
+
+    def layer(*args):
+        shapes = (args[0].shape[0], args[10].shape[1], args[10].shape[0], args[5].shape[0])
+        body = per_device
+        if fits(n_sp, n_tp, shapes):
+            body = functools.partial(split_hidden, n_sp, n_tp)
+        return jax.shard_map(
+            body, mesh=mesh, in_specs=in_specs, out_specs=out_specs, check_vma=False
+        )(*args)
+
+    return layer

time: 449 us -> 255 us (0.57)
  waiting for transfers between devices: 353 us -> 0 us
  Pallas kernels: 0 us -> 224 us
  blocking collectives: 50 us -> 0 us
  between operations: 14.3 us -> 0.8 us
  local copies, waits for them, and re-layouts: 1.36 us -> 11.5 us
  other arithmetic: 6.13 us -> 0.99 us
  matrix products: 22.3 us -> 17.2 us
    all_gather x5 -> x0, waiting for transfers between devices: 285 us -> none  [the longest x1 93.3 us: per_device(): lax.all_gather(down_weight, 'sp', axis=1, tiled=True)]
    pallas_call x0 -> x3, Pallas kernels: none -> 224 us  [the longest x1 114 us: spread(): pl.pallas_call(functools.partial(spread_kernel, n_sp, n_tp), out_shape=(j...]
    reduce_scatter x2 -> x0, waiting for transfers between devices: 66.1 us -> none  [the longest x1 39.9 us: per_device(): lax.psum_scatter(lax.dot_general(out_weight, attended, (((0,), (1,)), (()...]
    all_gather x2 -> x0, blocking collectives: 50 us -> none  [the longest x1 26.1 us: per_device(): key_first = lax.all_gather(keys_one, 'sp', axis=0, tiled=True)]
    slice x0 -> x1, local copies, waits for them, and re-layouts: none -> 6.04 us  [split_hidden(): gate_act = last_dot(normed, stacked[0])]
    dot_general x7, matrix products: 22.3 us -> 17.2 us  [the longest x1 7.93 us: split_hidden(): jnp.dot(hidden, stacked[2], preferred_element_type=jnp.float32)]
  transfers between devices with their start and end apart: 7 -> 0, of which waited for: 6 -> 0; matrix products, arithmetic and copies ran while one was open for 2% -> 0% of each run, Pallas kernels for 0% -> 0%
where the time goes in v1:
time: 255 us; the launch traced here: 254 us
  Pallas kernels  224 us (88%)
  matrix products  17.2 us (7%)
  local copies, waits for them, and re-layouts  11.5 us (5%)
    pallas_call x1, Pallas kernels, spread(): pl.pallas_call(functools.partial(spread_kernel, n_sp, n_tp), out_shape=(j...  114 us
    pallas_call x1, Pallas kernels, middle(): pl.pallas_call(functools.partial(middle_kernel, n_sp, n_tp), out_shape=(j...  62.8 us
    pallas_call x1, Pallas kernels, finish(): pl.pallas_call(functools.partial(finish_kernel, n_sp, n_tp), out_shape=ja...  46.6 us
    dot_general x1, matrix products, split_hidden(): jnp.dot(hidden, stacked[2], preferred_element_type=jnp.float32)  7.93 us
    dot_general x3, matrix products, last_dot(): lax.dot_general(left, right, (((1,), (1,)), ((), ())), preferred_element_...  6.43 us
    slice x1, local copies, waits for them, and re-layouts, split_hidden(): gate_act = last_dot(normed, stacked[0])  6.04 us
    unnamed x21, local copies, waits for them, and re-layouts  5.43 us

profile of v1, /device:TPU:13, one launch (start us, length us, event | category | flops | bytes accessed | tf_op | source)
XLA Modules:
  0.0 254.2 jit_solution(4432380392737549962)
XLA Ops:
  0.0 0.0 copy-start
  0.0 0.0 copy-start.1
  0.0 1.5 copy.15
  1.5 1.4 copy.14
  2.9 0.0 copy-done.1
  2.9 0.0 copy-start.2
  2.9 0.0 copy-start.3
  2.9 0.0 copy-start.4
  3.0 0.2 pad_maximum_fusion.w_ref
  3.2 0.6 copy-done.2
  3.8 0.0 copy-done.3
  3.8 0.0 copy-done.4
  3.9 114.3 %spread.1 = (bf16[3,4,176,2048]{3,2,1,0:T(8,128)(2,1)}, bf16[2048,512]{1,0:T(8,128)(2,1)S(1)}) custom-call(bf16[3,1408,256]{2,1,0:T(8,128)(2,1)S(1)} %pad_maximum_fusion.w_ref, bf16[256,512]{1,0:T(8,128)(2,1)S(1)} %pad_maximum_fusion.1.kv_ref), custom_call_target="tpu_custom_call" | custom-call | tf_op jit(solution)/shard_map/spread/pallas_call | solution.py:238
  118.2 0.0 copy-start.7
  118.2 6.0 %fusion.24 = (bf16[1,4,176,2048]{3,2,1,0:T(8,128)(2,1)}, bf16[1,4,176,2048]{3,2,1,0:T(8,128)(2,1)}, bf16[1,4,176,2048]{3,2,1,0:T(8,128)(2,1)}) fusion(bf16[3,4,176,2048]{3,2,1,0:T(8,128)(2,1)} %get-tuple-element.11), kind=kLoop, calls=%fused_computation.38 | loop fusion | bytes 17301504 | tf_op jit(solution)/shard_map/slice | solution.py:483
  124.2 0.0 copy-done.7
  124.2 0.5 fusion.25
  124.8 0.4 fusion.4
  125.1 0.0 copy-start.8
  125.1 0.7 convolution_divide_fusion.1
  125.8 0.2 copy-done.8
  126.0 0.5 fusion.26
  126.5 0.4 fusion.6
  127.5 0.0 copy-start.5
  127.5 0.7 multiply_reduce_fusion
  128.2 0.0 copy-done
  128.2 0.0 copy-done.5
  128.2 1.5 convolution_convert_fusion.1.part_ref
  129.8 62.8 %middle.1 = (bf16[64,2048]{1,0:T(8,128)(2,1)}, bf16[8,64,2048]{2,1,0:T(8,128)(2,1)}) custom-call(bf16[256,2048]{1,0:T(8,128)(2,1)} %convolution_convert_fusion.1.part_ref, bf16[256,512]{1,0:T(8,128)(2,1)} %res_ref.1, f32[1,2048]{1,0:T(1,128)} %bitcast.38), custom_call_target="tpu_custom_call" | custom-call | tf_op jit(solution)/shard_map/middle/pallas_call | solution.py:321
  192.6 0.0 copy-start.6
  192.6 5.4 %fusion.27 = f32[512,704]{0,1:T(8,128)} fusion(bf16[512,2048]{1,0:T(8,128)(2,1)} %bitcast.39, bf16[704,2048]{1,0:T(8,128)(2,1)} %bitcast.35), kind=kOutput, calls=%fused_computation.41 | convolution fusion | flops 1476395008 | bytes 6422528 | tf_op jit(solution)/shard_map/dot_general | solution.py:426
  198.0 0.0 copy-done.6
  198.0 7.9 %convolution_convert_fusion = bf16[512,2048]{1,0:T(8,128)(2,1)} fusion(bf16[704,2048]{1,0:T(8,128)(2,1)} %bitcast.33, bf16[512,2048]{1,0:T(8,128)(2,1)S(1)} %bitcast.40, bf16[704,2048]{1,0:T(8,128)(2,1)} %bitcast.34, f32[512,704]{0,1:T(8,128)} %fusion.27), kind=kOutput, calls=%fused_computation | convolution fusion | flops 2956001280 | bytes 11403264 | tf_op jit(solution)/shard_map/dot_general | solution.py:486
  205.9 46.6 %finish.1 = bf16[256,512]{1,0:T(8,128)(2,1)} custom-call(bf16[8,64,2048]{2,1,0:T(8,128)(2,1)} %bitcast.36, bf16[64,2048]{1,0:T(8,128)(2,1)} %get-tuple-element.12.resid_ref), custom_call_target="tpu_custom_call" | custom-call | tf_op jit(solution)/shard_map/finish/pallas_call | solution.py:406
  252.5 1.7 copy.18
  (3 shorter events, 0.0 us)
Async XLA Ops:
  0.0 128.2 %copy-start = (bf16[256,2048]{1,0:T(8,128)(2,1)S(1)}, bf16[256,2048]{1,0:T(8,128)(2,1)}, u32[]{:S(2)}) copy-start(bf16[256,2048]{1,0:T(8,128)(2,1)} %param.20) | copy-start | bytes 3145732
  0.0 2.9 %copy-start.1 = (bf16[1408,256]{1,0:T(8,128)(2,1)S(1)}, bf16[1408,256]{1,0:T(8,128)(2,1)}, u32[]{:S(2)}) copy-start(bf16[1408,256]{1,0:T(8,128)(2,1)} %param.25) | copy-start | bytes 2162692
  2.9 0.9 copy-start.2
  2.9 0.9 copy-start.3
  2.9 0.9 copy-start.4
  118.2 6.1 %copy-start.7 = (bf16[256,128]{1,0:T(8,128)(2,1)S(1)}, bf16[256,128]{1,0:T(8,128)(2,1)}, u32[]{:S(2)}) copy-start(bf16[256,128]{1,0:T(8,128)(2,1)} %param.13) | copy-start | bytes 196612
  125.1 0.8 copy-start.8
  127.5 0.7 copy-start.5
  192.6 5.4 %copy-start.6 = (bf16[8,64,2048]{2,1,0:T(8,128)(2,1)S(1)}, bf16[8,64,2048]{2,1,0:T(8,128)(2,1)}, u32[]{:S(2)}) copy-start(bf16[8,64,2048]{2,1,0:T(8,128)(2,1)} %get-tuple-element.10) | copy-start | bytes 6291460

commit v2 on v1

--- a/solution.py
+++ b/solution.py
@@ -162,15 +162,22 @@
     return s, t, y_peer, sibling, across
 
 
-def spread_kernel(n_sp, n_tp, w_ref, kv_ref, wall, kvall, *sems):
-    kv_s, kv_r, a_s, a_r, x_s, x_r, c_s, c_r, f_s, f_r, loc = sems
-    s, t, _, sibling, across = neighbours(n_sp, n_tp)
+def front_kernel(
+    n_sp, n_tp, w_ref, kv_ref, q1_ref, q2_ref, lam_ref, hgain_ref, ow_ref, res_ref, gain_ref,
+    wall, resid_ref, nall,
+    kvall, top, low, acc, part_ref, pbuf, rbuf, nbuf, *sems,
+):
+    (h_s, h_r, v_s, v_r, a_s, a_r, x_s, x_r, c_s, c_r, f_s, f_r, loc,
+     p_s, p_r, r_s, r_r, z_s, z_r, y_s, y_r) = sems
+    s, t, y_peer, sibling, across = neighbours(n_sp, n_tp)
+    z = lax.div(s, 2)
+    half = n_sp // 2
     rows = kv_ref.shape[0]
     part = w_ref.shape[1] // n_sp
     depth = w_ref.shape[2]
     greet(
         [{"sp": lax.rem(s + i, n_sp)} for i in range(1, n_sp)]
-        + [{"tp": sibling}, {"tp": across}]
+        + [{"tp": lax.rem(t + j, n_tp)} for j in range(1, n_tp)]
     )
 
     def block(who, source):
@@ -179,107 +186,184 @@
     def piece(dest):
         return w_ref.at[:, pl.ds(pl.multiple_of(dest * part, 16), part), :]
 
-    pending = []
-    kv_in, a_in = [], []
-    mine = kvall.at[pl.ds(pl.multiple_of(s * rows, rows), rows), :]
-    for i in range(1, n_sp):
-        copy = remote(kv_ref, mine, kv_s.at[i - 1], kv_r.at[i - 1], {"sp": lax.rem(s + i, n_sp)})
-        copy.start()
-        kv_in.append(copy)
-    for i in range(1, n_sp):
+    def weight(i):
         p = lax.rem(s + i, n_sp)
-        copy = remote(piece(p), block(t, s), a_s.at[i - 1], a_r.at[i - 1], {"sp": p})
-        copy.start()
-        a_in.append(copy)
-    own_kv = pltpu.make_async_copy(kv_ref, mine, loc.at[0])
+        return remote(piece(p), block(t, s), a_s.at[i - 1], a_r.at[i - 1], {"sp": p})
+
+    def kv_rows(who):
+        return kvall.at[pl.ds(pl.multiple_of(who * rows, rows), rows), :]
+
+    def hop(j):
+        who = s - 2 * j
+        src = kv_ref if j == 0 else kv_rows(who)
+        return remote(src, kv_rows(who), h_s.at[j], h_r.at[j], {"sp": lax.rem(s + 2, n_sp)})
+
+    def hop_in(j):
+        who = kv_rows(s - 2 - 2 * j)
+        return remote(who, who, h_s.at[j], h_r.at[j], {"sp": lax.rem(s + 2, n_sp)})
+
+    def over(j):
+        who = s - 2 * j
+        src = kv_ref if j == 0 else kv_rows(who)
+        return remote(src, kv_rows(who), v_s.at[j], v_r.at[j], {"sp": y_peer})
+
+    def over_in(j):
+        who = kv_rows(y_peer - 2 * j)
+        return remote(who, who, v_s.at[j], v_r.at[j], {"sp": y_peer})
+
+    own_kv = pltpu.make_async_copy(kv_ref, kv_rows(s), loc.at[0])
     own_kv.start()
     own_w = pltpu.make_async_copy(piece(s), block(t, s), loc.at[1])
     own_w.start()
-    x_in, c_in, f_in = [], [], []
-
-    def forward(i):
+
+    @pl.when(z < half - 1)
+    def _():
+        hop(0).start()
+
+    over(0).start()
+    even = list(range(2, n_sp, 2))
+    odd = list(range(1, n_sp, 2))
+    for i in even:
+
+        @pl.when(s + i >= n_sp)
+        def _(i=i):
+            weight(i).start()
+
+    for j in range(1, half):
+
+        @pl.when(z >= j)
+        def _(j=j):
+            hop_in(j - 1).wait_recv()
+            if j < half - 1:
+
+                @pl.when(z < half - 1)
+                def _():
+                    hop(j).start()
+
+            over(j).start()
+
+    for i in even:
+
+        @pl.when(s + i < n_sp)
+        def _(i=i):
+            weight(i).start()
+
+    for i in odd:
+        weight(i).start()
+
+    def across_copy(i):
         source = lax.rem(s - i + n_sp, n_sp)
-        remote(
+        return remote(
             block(t, source), block(t, source), x_s.at[i], x_r.at[i], {"tp": across}
-        ).wait_recv()
-        copy = remote(
+        )
+
+    def sibling_copy(i):
+        source = lax.rem(s - i + n_sp, n_sp)
+        return remote(
+            block(t, source), block(t, source), c_s.at[i], c_r.at[i], {"tp": sibling}
+        )
+
+    def second_copy(i):
+        source = lax.rem(s - i + n_sp, n_sp)
+        return remote(
             block(across, source), block(across, source), f_s.at[i], f_r.at[i], {"tp": sibling}
         )
-        copy.start()
-        f_in.append(copy)
-
-    for i in range(n_sp):
-        source = lax.rem(s - i + n_sp, n_sp)
+
+    def relay(i):
         if i == 0:
             own_w.wait()
         else:
-            a_in[i - 1].wait_recv()
-        for send, recv, where, into in ((x_s, x_r, across, x_in), (c_s, c_r, sibling, c_in)):
-            copy = remote(
-                block(t, source), block(t, source), send.at[i], recv.at[i], {"tp": where}
+            weight(i).wait_recv()
+        across_copy(i).start()
+        sibling_copy(i).start()
+
+    def second(i):
+        across_copy(i).wait_recv()
+        second_copy(i).start()
+
+    query_refs = (q1_ref, q2_ref)
+
+    def attend(j):
+        first = (z - j) * (2 * rows)
+        keys = pl.ds(pl.multiple_of(first, 2 * rows), 2 * rows)
+        for c in range(2):
+            scores = last_dot(
+                query_refs[c][...], kvall[keys, c * HEAD : (c + 1) * HEAD]
+            ) * HEAD ** (-0.5)
+            if j == 0:
+                query_pos = s * rows + lax.broadcasted_iota(jnp.int32, scores.shape, 0)
+                key_pos = first + lax.broadcasted_iota(jnp.int32, scores.shape, 1)
+                scores = jnp.where(key_pos <= query_pos, scores, masked_score)
+            highest = jnp.max(scores, axis=1, keepdims=True)
+            if j > 0:
+                highest = jnp.maximum(highest, top[c])
+            weights_exp = jnp.exp(scores - highest)
+            total = jnp.sum(weights_exp, axis=1, keepdims=True)
+            weighted = jnp.dot(
+                weights_exp.astype(jnp.bfloat16),
+                kvall[keys, 2 * HEAD :],
+                preferred_element_type=jnp.float32,
             )
-            copy.start()
-            into.append(copy)
-        if i >= 1:
-            forward(i - 1)
-    forward(n_sp - 1)
+            if j > 0:
+                keep = jnp.exp(top[c] - highest)
+                total = total + keep * low[c]
+                weighted = weighted + keep * acc[c]
+            top[c] = highest
+            low[c] = total
+            acc[c] = weighted
+
+    order = [0] + even + odd
     own_kv.wait()
-    for copy in kv_in:
-        copy.wait()
-    for copy in a_in + x_in:
-        copy.wait_send()
-    for copy in c_in + f_in:
-        copy.wait()
-
-
-def spread(weights, kv, n_sp, n_tp):
-    three, ff_here, depth = weights.shape
-    dma = pltpu.SemaphoreType.DMA
-    return pl.pallas_call(
-        functools.partial(spread_kernel, n_sp, n_tp),
-        out_shape=(
-            jax.ShapeDtypeStruct((three, n_tp, ff_here // n_sp, depth * n_sp), weights.dtype),
-            jax.ShapeDtypeStruct((kv.shape[0] * n_sp, kv.shape[1]), kv.dtype),
-        ),
-        in_specs=[pl.BlockSpec(memory_space=pltpu.VMEM)] * 2,
-        out_specs=[pl.BlockSpec(memory_space=pltpu.VMEM)] * 2,
-        scratch_shapes=[dma((n_sp - 1,))] * 4 + [dma((n_sp,))] * 6 + [dma((2,))],
-        compiler_params=pltpu.CompilerParams(
-            collective_id=0, has_side_effects=True, vmem_limit_bytes=48 * 2**20
-        ),
-        name="spread",
-    )(weights, kv)
-
-
-def middle_kernel(
-    n_sp, n_tp, part_ref, res_ref, gain_ref, resid_ref, nall, pbuf, rbuf, nbuf,
-    p_s, p_r, q_s, q_r, z_s, z_r, y_s, y_r,
-):
-    s, t, y_peer, _, _ = neighbours(n_sp, n_tp)
-    half = n_sp // 2
-    rows = nbuf.shape[0]
+    relay(order[0])
+    over_in(0).wait_recv()
+    attend(0)
+    done, crossed = 1, 0
+    for j in range(1, half):
+        relay(order[done])
+        done += 1
+
+        @pl.when(z >= j)
+        def _(j=j):
+            over_in(j).wait_recv()
+            attend(j)
+
+        second(order[crossed])
+        crossed += 1
+
+    mixed = acc[0] / low[0] - lam_ref[0, 0] * acc[1] / low[1]
+    mean_square = jnp.mean(mixed * mixed, axis=1, keepdims=True)
+    attended = (mixed * lax.rsqrt(mean_square + epsilon) * hgain_ref[...] * 0.8).astype(
+        jnp.bfloat16
+    )
+    width = ow_ref.shape[1]
+    for k in range(0, width, 512):
+        part_ref[:, k : k + 512] = jnp.dot(
+            attended, ow_ref[:, k : k + 512], preferred_element_type=jnp.float32
+        ).astype(jnp.bfloat16)
+
+    out_rows = nbuf.shape[0]
     cols = res_ref.shape[1]
-    greet(
-        [{"tp": lax.rem(t + j, n_tp)} for j in range(1, n_tp)]
-        + [{"sp": y_peer}]
-        + [{"sp": lax.rem(s + 2 * j, n_sp)} for j in range(1, half)]
-    )
     sent = []
 
     def take(p):
-        return pl.ds(pl.multiple_of(p * rows, rows), rows)
+        return pl.ds(pl.multiple_of(p * out_rows, out_rows), out_rows)
 
     here = pl.ds(pl.multiple_of(t * cols, cols), cols)
     for j in range(1, n_tp):
         p = lax.rem(t + j, n_tp)
         one = remote(part_ref.at[take(p), :], pbuf.at[j - 1], p_s.at[j - 1], p_r.at[j - 1], {"tp": p})
         two = remote(
-            res_ref.at[take(p), :], rbuf.at[:, here], q_s.at[j - 1], q_r.at[j - 1], {"tp": p}
+            res_ref.at[take(p), :], rbuf.at[:, here], r_s.at[j - 1], r_r.at[j - 1], {"tp": p}
         )
         one.start()
         two.start()
         sent += [one, two]
     rbuf[:, here] = res_ref[take(t), :]
+    while done < n_sp:
+        relay(order[done])
+        done += 1
+        second(order[crossed])
+        crossed += 1
     total = part_ref[take(t), :].astype(jnp.float32)
     for copy in sent:
         copy.wait()
@@ -292,16 +376,19 @@
     normed = (wide * lax.rsqrt(mean + epsilon) * gain_ref[...]).astype(jnp.bfloat16)
     nbuf[...] = normed
     z_in, y_in = [], []
+    copy = remote(nbuf, nall.at[s], y_s.at[0], y_r.at[0], {"sp": y_peer})
+    copy.start()
+    y_in.append(copy)
     for j in range(1, half):
         copy = remote(
             nbuf, nall.at[s], z_s.at[j - 1], z_r.at[j - 1], {"sp": lax.rem(s + 2 * j, n_sp)}
         )
         copy.start()
         z_in.append(copy)
-    copy = remote(nbuf, nall.at[s], y_s.at[0], y_r.at[0], {"sp": y_peer})
-    copy.start()
-    y_in.append(copy)
     nall[s] = normed
+    while crossed < n_sp:
+        second(order[crossed])
+        crossed += 1
     for j in range(1, half):
         z_in[j - 1].wait_recv()
         source = lax.rem(s - 2 * j + n_sp, n_sp)
@@ -312,31 +399,74 @@
         copy.wait_send()
     for copy in y_in:
         copy.wait()
-
-
-def middle(part, residual, gain, n_sp, n_tp):
-    rows, width = part.shape[0] // n_tp, part.shape[1]
+    for i in range(n_sp):
+        if i > 0:
+            weight(i).wait_send()
+        across_copy(i).wait_send()
+        sibling_copy(i).wait_send()
+        second_copy(i).wait_send()
+        source = lax.rem(s - i + n_sp, n_sp)
+        theirs = block(sibling, source)
+        remote(theirs, theirs, c_s.at[i], c_r.at[i], {"tp": sibling}).wait_recv()
+        theirs = block(lax.rem(sibling + 2, n_tp), source)
+        remote(theirs, theirs, f_s.at[i], f_r.at[i], {"tp": sibling}).wait_recv()
+    over(0).wait_send()
+
+    @pl.when(z < half - 1)
+    def _():
+        hop(0).wait_send()
+
+    for j in range(1, half):
+
+        @pl.when(z >= j)
+        def _(j=j):
+            over(j).wait_send()
+            if j < half - 1:
+
+                @pl.when(z < half - 1)
+                def _():
+                    hop(j).wait_send()
+
+
+def front(weights, kv, q1, q2, lam, hgain, ow, res, gain, n_sp, n_tp):
+    three, ff_here, depth = weights.shape
+    tok, width = kv.shape[0], ow.shape[1]
+    rows = tok // n_tp
+    half = n_sp // 2
     dma = pltpu.SemaphoreType.DMA
-    half = n_sp // 2
+    vmem = pl.BlockSpec(memory_space=pltpu.VMEM)
+    bf16, f32 = jnp.bfloat16, jnp.float32
     return pl.pallas_call(
-        functools.partial(middle_kernel, n_sp, n_tp),
+        functools.partial(front_kernel, n_sp, n_tp),
         out_shape=(
-            jax.ShapeDtypeStruct((rows, width), jnp.bfloat16),
-            jax.ShapeDtypeStruct((n_sp, rows, width), jnp.bfloat16),
+            jax.ShapeDtypeStruct((three, n_tp, ff_here // n_sp, depth * n_sp), bf16),
+            jax.ShapeDtypeStruct((rows, width), bf16),
+            jax.ShapeDtypeStruct((n_sp, rows, width), bf16),
         ),
-        in_specs=[pl.BlockSpec(memory_space=pltpu.VMEM)] * 3,
-        out_specs=[pl.BlockSpec(memory_space=pltpu.VMEM)] * 2,
+        in_specs=[vmem] * 4 + [pl.BlockSpec(memory_space=pltpu.SMEM)] + [vmem] * 4,
+        out_specs=[vmem] * 3,
         scratch_shapes=[
-            pltpu.VMEM((n_tp - 1, rows, width), jnp.bfloat16),
-            pltpu.VMEM((rows, width), jnp.bfloat16),
-            pltpu.VMEM((rows, width), jnp.bfloat16),
+            pltpu.VMEM((tok * n_sp, kv.shape[1]), bf16),
+            pltpu.VMEM((2, tok, 1), f32),
+            pltpu.VMEM((2, tok, 1), f32),
+            pltpu.VMEM((2, tok, ow.shape[0]), f32),
+            pltpu.VMEM((tok, width), bf16),
+            pltpu.VMEM((n_tp - 1, rows, width), bf16),
+            pltpu.VMEM((rows, width), bf16),
+            pltpu.VMEM((rows, width), bf16),
         ]
+        + [dma((half,))] * 4
+        + [dma((n_sp - 1,))] * 2
+        + [dma((n_sp,))] * 6
+        + [dma((2,))]
         + [dma((n_tp - 1,))] * 4
         + [dma((half - 1,))] * 2
         + [dma((half,))] * 2,
-        compiler_params=pltpu.CompilerParams(collective_id=1, has_side_effects=True),
-        name="middle",
-    )(part, residual, gain)
+        compiler_params=pltpu.CompilerParams(
+            collective_id=0, has_side_effects=True, vmem_limit_bytes=48 * 2**20
+        ),
+        name="front",
+    )(weights, kv, q1, q2, lam, hgain, ow, res, gain)
 
 
 def finish_kernel(
@@ -445,38 +575,21 @@
     up_weight,
     down_weight,
 ):
-    tok_rows = queries_one.shape[0]
     weights = jnp.stack([gate_weight.T, up_weight.T, down_weight])
     kv = jnp.concatenate([keys_one, keys_two, values], axis=1)
-    wall, kvall = spread(weights, kv, n_sp, n_tp)
-    query_pos = lax.axis_index("sp") * tok_rows + jnp.arange(tok_rows, dtype=jnp.int32)
-    key_pos = jnp.arange(kvall.shape[0], dtype=jnp.int32)
-    visible = key_pos[None, :] <= query_pos[:, None]
-    value_rows = kvall[:, 2 * HEAD :]
-
-    def one_map(queries, key_rows):
-        scores = last_dot(queries, key_rows) * HEAD ** (-0.5)
-        scores = jnp.where(visible, scores, masked_score)
-        weights_exp = jnp.exp(scores - jnp.max(scores, axis=1, keepdims=True))
-        totals = jnp.sum(weights_exp, axis=1, keepdims=True)
-        return (
-            jnp.dot(
-                weights_exp.astype(jnp.bfloat16), value_rows, preferred_element_type=jnp.float32
-            )
-            / totals
-        )
-
-    mixed = one_map(queries_one, kvall[:, :HEAD]) - mix_lambda[0] * one_map(
-        queries_two, kvall[:, HEAD : 2 * HEAD]
-    )
-    mean_square = jnp.mean(mixed * mixed, axis=1, keepdims=True)
-    attended = (mixed * lax.rsqrt(mean_square + epsilon) * head_gain[None, :] * 0.8).astype(
-        jnp.bfloat16
-    )
-    projected = jnp.dot(attended, out_weight, preferred_element_type=jnp.float32).astype(
-        jnp.bfloat16
-    )
-    resid, nall = middle(projected, residual_in, norm_gain[None, :], n_sp, n_tp)
+    wall, resid, nall = front(
+        weights,
+        kv,
+        queries_one,
+        queries_two,
+        mix_lambda[None, :],
+        head_gain[None, :],
+        out_weight,
+        residual_in,
+        norm_gain[None, :],
+        n_sp,
+        n_tp,
+    )
     width = nall.shape[2]
     normed = nall.reshape(-1, width)
     stacked = wall.reshape(3, -1, width)

time: 255 us -> 186 us (0.73)
  Pallas kernels: 224 us -> 161 us
  matrix products: 17.2 us -> 9.17 us
  other arithmetic: 0.99 us -> 3.82 us
    pallas_call x2 -> x1, Pallas kernels: 177 us -> 111 us  [front(): pl.pallas_call(functools.partial(front_kernel, n_sp, n_tp), out_shape=(ja...]
    dot_general x3 -> x1, matrix products: 6.43 us -> 1.68 us  [last_dot(): lax.dot_general(left, right, (((1,), (1,)), ((), ())), preferred_element_...]
    pallas_call x1, Pallas kernels: 46.6 us -> 50.7 us  [finish(): pl.pallas_call(functools.partial(finish_kernel, n_sp, n_tp), out_shape=ja...]
    dot_general x3 -> x0, matrix products: 2.88 us -> none  [the longest x1 1.55 us: split_hidden(): jnp.dot(attended, out_weight, preferred_element_type=jnp.float32)]
    another operation x1, other arithmetic: 0.24 us -> 2.85 us  [split_hidden(): weights = jnp.stack([gate_weight.T, up_weight.T, down_weight])]
    unnamed x21 -> x19, local copies, waits for them, and re-layouts: 5.43 us -> 3.38 us
where the time goes in v2:
time: 186 us; the launch traced here: 184 us
  Pallas kernels  161 us (87%)
  matrix products  9.17 us (5%)
  local copies, waits for them, and re-layouts  9.06 us (5%)
  other arithmetic  3.82 us (2%)
    pallas_call x1, Pallas kernels, front(): pl.pallas_call(functools.partial(front_kernel, n_sp, n_tp), out_shape=(ja...  111 us
    pallas_call x1, Pallas kernels, finish(): pl.pallas_call(functools.partial(finish_kernel, n_sp, n_tp), out_shape=ja...  50.7 us
    dot_general x1, matrix products, split_hidden(): jnp.dot(hidden, stacked[2], preferred_element_type=jnp.float32)  7.49 us
    slice x1, local copies, waits for them, and re-layouts, split_hidden(): gate_act = last_dot(normed, stacked[0])  5.68 us

profile of v2, /device:TPU:13, one launch (start us, length us, event | category | flops | bytes accessed | tf_op | source)
XLA Modules:
  0.0 184.4 jit_solution(9916761827394929080)
XLA Ops:
  0.0 0.0 copy-start.7
  0.7 1.0 pad_maximum_fusion.1.kv_ref
  1.7 1.4 copy.14
  3.1 0.0 copy-done.7
  3.1 0.3 copy.15
  3.4 0.0 copy-start
  3.4 0.0 copy-start.1
  3.4 0.0 copy-start.3
  3.4 0.0 copy-start.4
  3.4 0.0 copy-start.5
  3.4 0.0 copy-start.6
  3.4 2.8 %pad_maximum_fusion.w_ref = bf16[3,1408,256]{2,1,0:T(8,128)(2,1)} fusion(bf16[1,1408,256]{2,1,0:T(8,128)(2,1)} %bitcast.31, bf16[1,1408,256]{2,1,0:T(8,128)(2,1)S(1)} %bitcast.26, bf16[1,1408,256]{2,1,0:T(8,128)(2,1)S(1)} %bitcast.25), kind=kLoop, calls=%fused_computation.1 | loop fusion | flops 2162688 | bytes 4325376 | tf_op jit(solution)/shard_map/stack | solution.py:578
  6.3 0.0 copy-done
  6.3 0.0 copy-done.1
  6.3 0.0 copy-done.3
  6.3 0.0 copy-done.4
  6.3 0.0 copy-done.5
  6.3 0.0 copy-done.6
  6.3 110.8 %front.1 = (bf16[3,4,176,2048]{3,2,1,0:T(8,128)(2,1)}, bf16[64,2048]{1,0:T(8,128)(2,1)S(1)}, bf16[8,64,2048]{2,1,0:T(8,128)(2,1)S(1)}) custom-call(bf16[3,1408,256]{2,1,0:T(8,128)(2,1)} %pad_maximum_fusion.w_ref, bf16[256,512]{1,0:T(8,128)(2,1)S(1)} %pad_maximum_fusion.1.kv_ref, bf16[256,128]{1,0:T(8,128)(2,1)S(1)} %copy-done.3, ...), custom_call_target="tpu_custom_call" | custom-call | tf_op jit(solution)/shard_map/front/pallas_call | solution.py:439
  117.1 0.0 copy-start.2
  117.1 5.7 %fusion.2 = (bf16[1,4,176,2048]{3,2,1,0:T(8,128)(2,1)S(1)}, bf16[1,4,176,2048]{3,2,1,0:T(8,128)(2,1)}, bf16[1,4,176,2048]{3,2,1,0:T(8,128)(2,1)}) fusion(bf16[3,4,176,2048]{3,2,1,0:T(8,128)(2,1)} %get-tuple-element.9), kind=kLoop, calls=%fused_computation.6 | loop fusion | bytes 17301504 | tf_op jit(solution)/shard_map/slice | solution.py:596
  122.8 0.0 copy-done.2
  122.8 1.7 fusion.3
  124.5 7.5 %convolution_convert_fusion = bf16[512,2048]{1,0:T(8,128)(2,1)} fusion(bf16[704,2048]{1,0:T(8,128)(2,1)} %bitcast.27, bf16[512,2048]{1,0:T(8,128)(2,1)S(1)} %bitcast.24, bf16[704,2048]{1,0:T(8,128)(2,1)} %bitcast.28, f32[512,704]{0,1:T(8,128)S(1)} %fusion.3), kind=kOutput, calls=%fused_computation | convolution fusion | flops 2956001280 | bytes 11403264 | tf_op jit(solution)/shard_map/dot_general | solution.py:599
  132.0 50.7 %finish.1 = bf16[256,512]{1,0:T(8,128)(2,1)} custom-call(bf16[8,64,2048]{2,1,0:T(8,128)(2,1)} %bitcast.30, bf16[64,2048]{1,0:T(8,128)(2,1)} %copy-done.2), custom_call_target="tpu_custom_call" | custom-call | tf_op jit(solution)/shard_map/finish/pallas_call | solution.py:536
  182.7 1.7 copy.18
Async XLA Ops:
  0.0 3.1 %copy-start.7 = (bf16[256,1408]{1,0:T(8,128)(2,1)S(1)}, bf16[256,1408]{1,0:T(8,128)(2,1)}, u32[]{:S(2)}) copy-start(bf16[256,1408]{1,0:T(8,128)(2,1)} %param.24) | copy-start | bytes 2162692
  3.4 2.9 %copy-start = (bf16[256,2048]{1,0:T(8,128)(2,1)S(1)}, bf16[256,2048]{1,0:T(8,128)(2,1)}, u32[]{:S(2)}) copy-start(bf16[256,2048]{1,0:T(8,128)(2,1)} %ow_ref.1) | copy-start | bytes 3145732
  3.4 2.9 %copy-start.1 = (bf16[256,512]{1,0:T(8,128)(2,1)S(1)}, bf16[256,512]{1,0:T(8,128)(2,1)}, u32[]{:S(2)}) copy-start(bf16[256,512]{1,0:T(8,128)(2,1)} %res_ref.1) | copy-start | bytes 786436
  3.4 2.9 %copy-start.3 = (bf16[256,128]{1,0:T(8,128)(2,1)S(1)}, bf16[256,128]{1,0:T(8,128)(2,1)}, u32[]{:S(2)}) copy-start(bf16[256,128]{1,0:T(8,128)(2,1)} %q1_ref.1) | copy-start | bytes 196612
  3.4 2.9 %copy-start.4 = (bf16[256,128]{1,0:T(8,128)(2,1)S(1)}, bf16[256,128]{1,0:T(8,128)(2,1)}, u32[]{:S(2)}) copy-start(bf16[256,128]{1,0:T(8,128)(2,1)} %q2_ref.1) | copy-start | bytes 196612
  3.4 2.9 %copy-start.5 = (f32[2048]{0:T(1024)S(1)}, f32[2048]{0:T(1024)}, u32[]{:S(2)}) copy-start(f32[2048]{0:T(1024)} %param.22) | copy-start | bytes 24580
  3.4 2.9 %copy-start.6 = (f32[256]{0:T(256)S(1)}, f32[256]{0:T(256)}, u32[]{:S(2)}) copy-start(f32[256]{0:T(256)} %param.19) | copy-start | bytes 3076
  117.1 5.7 %copy-start.2 = (bf16[64,2048]{1,0:T(8,128)(2,1)}, bf16[64,2048]{1,0:T(8,128)(2,1)S(1)}, u32[]{:S(2)}) copy-start(bf16[64,2048]{1,0:T(8,128)(2,1)S(1)} %get-tuple-element.10.resid_ref) | copy-start | bytes 786436

commit v3 on v2

--- a/solution.py
+++ b/solution.py
@@ -164,13 +164,14 @@
 
 def front_kernel(
     n_sp, n_tp, w_ref, kv_ref, q1_ref, q2_ref, lam_ref, hgain_ref, ow_ref, res_ref, gain_ref,
-    wall, resid_ref, nall,
+    out_ref,
+    wall, resid_ref, nall, part2, ybuf, cbuf, zbuf, fbuf,
     kvall, top, low, acc, part_ref, pbuf, rbuf, nbuf, *sems,
 ):
     (h_s, h_r, v_s, v_r, a_s, a_r, x_s, x_r, c_s, c_r, f_s, f_r, loc,
-     p_s, p_r, r_s, r_r, z_s, z_r, y_s, y_r) = sems
+     p_s, p_r, r_s, r_r, z_s, z_r, y_s, y_r, e_s, e_r, g_s, g_r, o_s, o_r) = sems
     s, t, y_peer, sibling, across = neighbours(n_sp, n_tp)
-    z = lax.div(s, 2)
+    z, y = lax.div(s, 2), lax.rem(s, 2)
     half = n_sp // 2
     rows = kv_ref.shape[0]
     part = w_ref.shape[1] // n_sp
@@ -359,7 +360,7 @@
         two.start()
         sent += [one, two]
     rbuf[:, here] = res_ref[take(t), :]
-    while done < n_sp:
+    while done < n_sp - 2:
         relay(order[done])
         done += 1
         second(order[crossed])
@@ -376,28 +377,95 @@
     normed = (wide * lax.rsqrt(mean + epsilon) * gain_ref[...]).astype(jnp.bfloat16)
     nbuf[...] = normed
     z_in, y_in = [], []
-    copy = remote(nbuf, nall.at[s], y_s.at[0], y_r.at[0], {"sp": y_peer})
+    copy = remote(nbuf, nall.at[y, z], y_s.at[0], y_r.at[0], {"sp": y_peer})
     copy.start()
     y_in.append(copy)
     for j in range(1, half):
         copy = remote(
-            nbuf, nall.at[s], z_s.at[j - 1], z_r.at[j - 1], {"sp": lax.rem(s + 2 * j, n_sp)}
+            nbuf, nall.at[y, z], z_s.at[j - 1], z_r.at[j - 1], {"sp": lax.rem(s + 2 * j, n_sp)}
         )
         copy.start()
         z_in.append(copy)
-    nall[s] = normed
+    nall[y, z] = normed
     while crossed < n_sp:
+        if done < n_sp:
+            relay(order[done])
+            done += 1
         second(order[crossed])
         crossed += 1
     for j in range(1, half):
         z_in[j - 1].wait_recv()
-        source = lax.rem(s - 2 * j + n_sp, n_sp)
-        copy = remote(nall.at[source], nall.at[source], y_s.at[j], y_r.at[j], {"sp": y_peer})
+        held = nall.at[y, lax.rem(z - j + half, half)]
+        copy = remote(held, held, y_s.at[j], y_r.at[j], {"sp": y_peer})
         copy.start()
         y_in.append(copy)
-    for copy in z_in:
+    for i in range(n_sp):
+        source = lax.rem(s - i + n_sp, n_sp)
+        theirs = block(sibling, source)
+        remote(theirs, theirs, c_s.at[i], c_r.at[i], {"tp": sibling}).wait_recv()
+        theirs = block(lax.rem(sibling + 2, n_tp), source)
+        remote(theirs, theirs, f_s.at[i], f_r.at[i], {"tp": sibling}).wait_recv()
+
+    units = n_tp * part
+
+    def mixer(parity, slot):
+        tokens = nall[parity].reshape(half * out_rows, width)
+        gate_act = last_dot(tokens, wall[0].reshape(units, width))
+        up_act = last_dot(tokens, wall[1].reshape(units, width))
+        hidden = (gate_act / (1.0 + jnp.exp(-gate_act)) * up_act).astype(jnp.bfloat16)
+        for k in range(0, width, 512):
+            product = jnp.dot(
+                hidden,
+                wall[2, :, :, k : k + 512].reshape(units, 512),
+                preferred_element_type=jnp.float32,
+            ).astype(jnp.bfloat16)
+            part2[slot, :, :, k : k + 512] = product.reshape(half, out_rows, 512)
+
+    mixer(y, 0)
+    for copy in y_in:
+        copy.wait_recv()
+    mixer(1 - y, 1)
+    turn = list(range(1, half)) + [0]
+    e_in = {}
+    for j in turn:
+        zi = lax.rem(z + j, half)
+        copy = remote(part2.at[1, zi], ybuf.at[j], e_s.at[j], e_r.at[j], {"sp": y_peer})
+        copy.start()
+        e_in[j] = copy
+    g_in = []
+    for j in turn:
+        e_in[j].wait_recv()
+        both = part2[0, lax.rem(z + j, half)].astype(jnp.float32) + ybuf[j].astype(jnp.float32)
+        if j == 0:
+            total = both
+        else:
+            cbuf[j - 1] = both.astype(jnp.bfloat16)
+            copy = remote(
+                cbuf.at[j - 1], zbuf.at[j - 1], g_s.at[j - 1], g_r.at[j - 1],
+                {"sp": lax.rem(s + 2 * j, n_sp)},
+            )
+            copy.start()
+            g_in.append(copy)
+    for copy in g_in:
+        copy.wait_recv()
+    for j in range(1, half):
+        total = total + zbuf[j - 1].astype(jnp.float32)
+    fbuf[...] = (resid_ref[...].astype(jnp.float32) + total).astype(jnp.bfloat16)
+    o_in = []
+    for j in range(1, n_tp):
+        p = lax.rem(t + j, n_tp)
+        copy = remote(
+            fbuf.at[:, pl.ds(pl.multiple_of(p * cols, cols), cols)], out_ref.at[take(t), :],
+            o_s.at[j - 1], o_r.at[j - 1], {"tp": p},
+        )
+        copy.start()
+        o_in.append(copy)
+    out_ref[take(t), :] = fbuf[:, here]
+    for copy in z_in + y_in + g_in:
         copy.wait_send()
-    for copy in y_in:
+    for j in turn:
+        e_in[j].wait_send()
+    for copy in o_in:
         copy.wait()
     for i in range(n_sp):
         if i > 0:
@@ -405,11 +473,6 @@
         across_copy(i).wait_send()
         sibling_copy(i).wait_send()
         second_copy(i).wait_send()
-        source = lax.rem(s - i + n_sp, n_sp)
-        theirs = block(sibling, source)
-        remote(theirs, theirs, c_s.at[i], c_r.at[i], {"tp": sibling}).wait_recv()
-        theirs = block(lax.rem(sibling + 2, n_tp), source)
-        remote(theirs, theirs, f_s.at[i], f_r.at[i], {"tp": sibling}).wait_recv()
     over(0).wait_send()
 
     @pl.when(z < half - 1)
@@ -436,24 +499,29 @@
     dma = pltpu.SemaphoreType.DMA
     vmem = pl.BlockSpec(memory_space=pltpu.VMEM)
     bf16, f32 = jnp.bfloat16, jnp.float32
+    rowblock = (rows, width)
     return pl.pallas_call(
         functools.partial(front_kernel, n_sp, n_tp),
-        out_shape=(
-            jax.ShapeDtypeStruct((three, n_tp, ff_here // n_sp, depth * n_sp), bf16),
-            jax.ShapeDtypeStruct((rows, width), bf16),
-            jax.ShapeDtypeStruct((n_sp, rows, width), bf16),
-        ),
+        out_shape=jax.ShapeDtypeStruct((tok, width // n_tp), bf16),
         in_specs=[vmem] * 4 + [pl.BlockSpec(memory_space=pltpu.SMEM)] + [vmem] * 4,
-        out_specs=[vmem] * 3,
+        out_specs=vmem,
         scratch_shapes=[
+            pltpu.VMEM((three, n_tp, ff_here // n_sp, depth * n_sp), bf16),
+            pltpu.VMEM(rowblock, bf16),
+            pltpu.VMEM((2, half) + rowblock, bf16),
+            pltpu.VMEM((2, half) + rowblock, bf16),
+            pltpu.VMEM((half,) + rowblock, bf16),
+            pltpu.VMEM((half - 1,) + rowblock, bf16),
+            pltpu.VMEM((half - 1,) + rowblock, bf16),
+            pltpu.VMEM(rowblock, bf16),
             pltpu.VMEM((tok * n_sp, kv.shape[1]), bf16),
             pltpu.VMEM((2, tok, 1), f32),
             pltpu.VMEM((2, tok, 1), f32),
             pltpu.VMEM((2, tok, ow.shape[0]), f32),
             pltpu.VMEM((tok, width), bf16),
-            pltpu.VMEM((n_tp - 1, rows, width), bf16),
-            pltpu.VMEM((rows, width), bf16),
-            pltpu.VMEM((rows, width), bf16),
+            pltpu.VMEM((n_tp - 1,) + rowblock, bf16),
+            pltpu.VMEM(rowblock, bf16),
+            pltpu.VMEM(rowblock, bf16),
         ]
         + [dma((half,))] * 4
         + [dma((n_sp - 1,))] * 2
@@ -461,95 +529,14 @@
         + [dma((2,))]
         + [dma((n_tp - 1,))] * 4
         + [dma((half - 1,))] * 2
-        + [dma((half,))] * 2,
+        + [dma((half,))] * 4
+        + [dma((half - 1,))] * 2
+        + [dma((n_tp - 1,))] * 2,
         compiler_params=pltpu.CompilerParams(
-            collective_id=0, has_side_effects=True, vmem_limit_bytes=48 * 2**20
+            collective_id=0, has_side_effects=True, vmem_limit_bytes=56 * 2**20
         ),
         name="front",
     )(weights, kv, q1, q2, lam, hgain, ow, res, gain)
-
-
-def finish_kernel(
-    n_sp, n_tp, part_ref, resid_ref, out_ref, ybuf, cbuf, zbuf, fbuf,
-    y_s, y_r, z_s, z_r, o_s, o_r,
-):
-    s, t, y_peer, _, _ = neighbours(n_sp, n_tp)
-    half = n_sp // 2
-    rows = fbuf.shape[0]
-    cols = out_ref.shape[1]
-    greet(
-        [{"tp": lax.rem(t + j, n_tp)} for j in range(1, n_tp)]
-        + [{"sp": y_peer}]
-        + [{"sp": lax.rem(s + 2 * j, n_sp)} for j in range(1, half)]
-    )
-    order = list(range(1, half)) + [0]
-    y_in = {}
-    for j in order:
-        copy = remote(
-            part_ref.at[lax.rem(y_peer + 2 * j, n_sp)], ybuf.at[j], y_s.at[j], y_r.at[j],
-            {"sp": y_peer},
-        )
-        copy.start()
-        y_in[j] = copy
-    z_in = []
-    for j in order:
-        y_in[j].wait_recv()
-        both = part_ref[lax.rem(s + 2 * j, n_sp)].astype(jnp.float32) + ybuf[j].astype(jnp.float32)
-        if j == 0:
-            total = both
-        else:
-            cbuf[j - 1] = both.astype(jnp.bfloat16)
-            copy = remote(
-                cbuf.at[j - 1], zbuf.at[j - 1], z_s.at[j - 1], z_r.at[j - 1],
-                {"sp": lax.rem(s + 2 * j, n_sp)},
-            )
-            copy.start()
-            z_in.append(copy)
-    for j in range(1, half):
-        z_in[j - 1].wait_recv()
-        total = total + zbuf[j - 1].astype(jnp.float32)
-    fbuf[...] = (resid_ref[...].astype(jnp.float32) + total).astype(jnp.bfloat16)
-    mine = pl.ds(pl.multiple_of(t * rows, rows), rows)
-    out = []
-    for j in range(1, n_tp):
-        p = lax.rem(t + j, n_tp)
-        copy = remote(
-            fbuf.at[:, pl.ds(pl.multiple_of(p * cols, cols), cols)], out_ref.at[mine, :],
-            o_s.at[j - 1], o_r.at[j - 1], {"tp": p},
-        )
-        copy.start()
-        out.append(copy)
-    out_ref[mine, :] = fbuf[:, pl.ds(pl.multiple_of(t * cols, cols), cols)]
-    for copy in out:
-        copy.wait()
-    for j in order:
-        y_in[j].wait_send()
-    for copy in z_in:
-        copy.wait_send()
-
-
-def finish(part, resid, n_sp, n_tp):
-    _, rows, width = part.shape
-    dma = pltpu.SemaphoreType.DMA
-    half = n_sp // 2
-    block = (rows, width)
-    return pl.pallas_call(
-        functools.partial(finish_kernel, n_sp, n_tp),
-        out_shape=jax.ShapeDtypeStruct((rows * n_tp, width // n_tp), jnp.bfloat16),
-        in_specs=[pl.BlockSpec(memory_space=pltpu.VMEM)] * 2,
-        out_specs=pl.BlockSpec(memory_space=pltpu.VMEM),
-        scratch_shapes=[
-            pltpu.VMEM((half,) + block, jnp.bfloat16),
-            pltpu.VMEM((half - 1,) + block, jnp.bfloat16),
-            pltpu.VMEM((half - 1,) + block, jnp.bfloat16),
-            pltpu.VMEM(block, jnp.bfloat16),
-        ]
-        + [dma((half,))] * 2
-        + [dma((half - 1,))] * 2
-        + [dma((n_tp - 1,))] * 2,
-        compiler_params=pltpu.CompilerParams(collective_id=2, has_side_effects=True),
-        name="finish",
-    )(part, resid)
 
 
 def last_dot(left, right):
@@ -577,7 +564,7 @@
 ):
     weights = jnp.stack([gate_weight.T, up_weight.T, down_weight])
     kv = jnp.concatenate([keys_one, keys_two, values], axis=1)
-    wall, resid, nall = front(
+    return front(
         weights,
         kv,
         queries_one,
@@ -590,14 +577,6 @@
         n_sp,
         n_tp,
     )
-    width = nall.shape[2]
-    normed = nall.reshape(-1, width)
-    stacked = wall.reshape(3, -1, width)
-    gate_act = last_dot(normed, stacked[0])
-    up_act = last_dot(normed, stacked[1])
-    hidden = (jax.nn.silu(gate_act) * up_act).astype(jnp.bfloat16)
-    partials = jnp.dot(hidden, stacked[2], preferred_element_type=jnp.float32).astype(jnp.bfloat16)
-    return finish(partials.reshape(nall.shape), resid, n_sp, n_tp)
 
 
 def fits(n_sp, n_tp, shapes):

time: 186 us -> 158 us (0.85)
  Pallas kernels: 161 us -> 149 us
  matrix products: 9.17 us -> 0 us
  local copies, waits for them, and re-layouts: 9.06 us -> 4.52 us
    pallas_call x2 -> x1, Pallas kernels: 161 us -> 149 us  [front(): pl.pallas_call(functools.partial(front_kernel, n_sp, n_tp), out_shape=jax...]
    dot_general x2 -> x0, matrix products: 9.17 us -> none  [the longest x1 7.49 us: split_hidden(): jnp.dot(hidden, stacked[2], preferred_element_type=jnp.float32)]
    slice x1 -> x0, local copies, waits for them, and re-layouts: 5.68 us -> none  [split_hidden(): gate_act = last_dot(normed, stacked[0])]
    unnamed x19 -> x11, local copies, waits for them, and re-layouts: 3.38 us -> 4.52 us
where the time goes in v3:
time: 158 us; the launch traced here: 157 us
  Pallas kernels  149 us (94%)
  local copies, waits for them, and re-layouts  4.52 us (3%)
  other arithmetic  2.33 us (1%)
    pallas_call x1, Pallas kernels, front(): pl.pallas_call(functools.partial(front_kernel, n_sp, n_tp), out_shape=jax...  149 us
    unnamed x11, local copies, waits for them, and re-layouts  4.52 us

profile of v3, /device:TPU:13, one launch (start us, length us, event | category | flops | bytes accessed | tf_op | source)
XLA Modules:
  0.0 156.8 jit_solution(4284129491270865989)
XLA Ops:
  0.0 0.0 copy-start
  0.0 1.4 copy.14
  1.5 1.4 copy.15
  2.8 0.0 copy-done
  2.9 0.0 copy-start.1
  2.9 0.0 copy-start.2
  2.9 0.0 copy-start.3
  2.9 1.6 %pad_maximum_fusion.w_ref = bf16[3,1408,256]{2,1,0:T(8,128)(2,1)} fusion(bf16[1,1408,256]{2,1,0:T(8,128)(2,1)S(1)} %bitcast.13, bf16[1,1408,256]{2,1,0:T(8,128)(2,1)S(1)} %bitcast.12, bf16[1,1408,256]{2,1,0:T(8,128)(2,1)S(1)} %bitcast.11), kind=kLoop, calls=%fused_computation | loop fusion | flops 2162688 | bytes 4325376 | tf_op jit(solution)/shard_map/stack | solution.py:565
  4.5 0.0 copy-done.1
  4.5 0.0 copy-done.2
  4.5 0.0 copy-done.3
  4.5 0.7 pad_maximum_fusion.1.kv_ref
  5.9 149.2 %front.1 = bf16[256,512]{1,0:T(8,128)(2,1)} custom-call(bf16[3,1408,256]{2,1,0:T(8,128)(2,1)} %pad_maximum_fusion.w_ref, bf16[256,512]{1,0:T(8,128)(2,1)} %pad_maximum_fusion.1.kv_ref, bf16[256,128]{1,0:T(8,128)(2,1)} %q1_ref.1, bf16[256,128]{1,0:T(8,128)(2,1)} %q2_ref.1, f32[1,1]{1,0:T(1,128)} %bitcast.10.lam_ref, f32[1,256]{1,0:T(1,128)} %bitcast.15, ...), custom_call_target="tpu_custom_call" | custom-call | tf_op jit(solution)/shard_map/front/pallas_call | solution.py:503
  155.1 1.7 %copy.18 = bf16[256,512]{1,0:T(8,128)(2,1)} copy(bf16[256,512]{1,0:T(8,128)(2,1)} %front.1) | data formatting | bytes 524288
Async XLA Ops:
  0.0 2.8 %copy-start = (bf16[1408,256]{1,0:T(8,128)(2,1)S(1)}, bf16[1408,256]{1,0:T(8,128)(2,1)}, u32[]{:S(2)}) copy-start(bf16[1408,256]{1,0:T(8,128)(2,1)} %param.25) | copy-start | bytes 2162692
  2.9 1.6 %copy-start.1 = (bf16[256,256]{1,0:T(8,128)(2,1)S(1)}, bf16[256,256]{1,0:T(8,128)(2,1)}, u32[]{:S(2)}) copy-start(bf16[256,256]{1,0:T(8,128)(2,1)} %param.17) | copy-start | bytes 393220
  2.9 1.6 %copy-start.2 = (bf16[256,128]{1,0:T(8,128)(2,1)S(1)}, bf16[256,128]{1,0:T(8,128)(2,1)}, u32[]{:S(2)}) copy-start(bf16[256,128]{1,0:T(8,128)(2,1)} %param.16) | copy-start | bytes 196612
  2.9 1.6 %copy-start.3 = (bf16[256,128]{1,0:T(8,128)(2,1)S(1)}, bf16[256,128]{1,0:T(8,128)(2,1)}, u32[]{:S(2)}) copy-start(bf16[256,128]{1,0:T(8,128)(2,1)} %param.15) | copy-start | bytes 196612

commit v4 on v3

--- a/solution.py
+++ b/solution.py
@@ -165,7 +165,7 @@
 def front_kernel(
     n_sp, n_tp, w_ref, kv_ref, q1_ref, q2_ref, lam_ref, hgain_ref, ow_ref, res_ref, gain_ref,
     out_ref,
-    wall, resid_ref, nall, part2, ybuf, cbuf, zbuf, fbuf,
+    wall, resid_ref, nall, hidden, part2, ybuf, cbuf, zbuf, fbuf,
     kvall, top, low, acc, part_ref, pbuf, rbuf, nbuf, *sems,
 ):
     (h_s, h_r, v_s, v_r, a_s, a_r, x_s, x_r, c_s, c_r, f_s, f_r, loc,
@@ -181,15 +181,19 @@
         + [{"tp": lax.rem(t + j, n_tp)} for j in range(1, n_tp)]
     )
 
-    def block(who, source):
-        return wall.at[:, who, :, pl.ds(pl.multiple_of(source * depth, depth), depth)]
-
-    def piece(dest):
-        return w_ref.at[:, pl.ds(pl.multiple_of(dest * part, 16), part), :]
-
-    def weight(i):
+    def block(who, source, w):
+        columns = pl.ds(pl.multiple_of(source * depth, depth), depth)
+        return wall.at[pl.ds(2 * w, 2 - w), who, :, columns]
+
+    def piece(dest, w):
+        units_there = pl.ds(pl.multiple_of(dest * part, 16), part)
+        return w_ref.at[pl.ds(2 * w, 2 - w), units_there, :]
+
+    def weight(i, w):
         p = lax.rem(s + i, n_sp)
-        return remote(piece(p), block(t, s), a_s.at[i - 1], a_r.at[i - 1], {"sp": p})
+        return remote(
+            piece(p, w), block(t, s, w), a_s.at[w, i - 1], a_r.at[w, i - 1], {"sp": p}
+        )
 
     def kv_rows(who):
         return kvall.at[pl.ds(pl.multiple_of(who * rows, rows), rows), :]
@@ -214,8 +218,11 @@
 
     own_kv = pltpu.make_async_copy(kv_ref, kv_rows(s), loc.at[0])
     own_kv.start()
-    own_w = pltpu.make_async_copy(piece(s), block(t, s), loc.at[1])
-    own_w.start()
+    own_w = [
+        pltpu.make_async_copy(piece(s, w), block(t, s, w), loc.at[1 + w]) for w in range(2)
+    ]
+    for copy in own_w:
+        copy.start()
 
     @pl.when(z < half - 1)
     def _():
@@ -228,7 +235,7 @@
 
         @pl.when(s + i >= n_sp)
         def _(i=i):
-            weight(i).start()
+            weight(i, 0).start()
 
     for j in range(1, half):
 
@@ -247,40 +254,46 @@
 
         @pl.when(s + i < n_sp)
         def _(i=i):
-            weight(i).start()
+            weight(i, 0).start()
 
     for i in odd:
-        weight(i).start()
-
-    def across_copy(i):
+        weight(i, 0).start()
+
+    def across_copy(i, w):
         source = lax.rem(s - i + n_sp, n_sp)
         return remote(
-            block(t, source), block(t, source), x_s.at[i], x_r.at[i], {"tp": across}
-        )
-
-    def sibling_copy(i):
+            block(t, source, w), block(t, source, w), x_s.at[w, i], x_r.at[w, i], {"tp": across}
+        )
+
+    def sibling_copy(i, w):
         source = lax.rem(s - i + n_sp, n_sp)
         return remote(
-            block(t, source), block(t, source), c_s.at[i], c_r.at[i], {"tp": sibling}
-        )
-
-    def second_copy(i):
-        source = lax.rem(s - i + n_sp, n_sp)
-        return remote(
-            block(across, source), block(across, source), f_s.at[i], f_r.at[i], {"tp": sibling}
-        )
-
-    def relay(i):
+            block(t, source, w), block(t, source, w), c_s.at[w, i], c_r.at[w, i], {"tp": sibling}
+        )
+
+    def second_copy(i, w):
+        held = block(across, lax.rem(s - i + n_sp, n_sp), w)
+        return remote(held, held, f_s.at[w, i], f_r.at[w, i], {"tp": sibling})
+
+    def relay(i, w):
         if i == 0:
-            own_w.wait()
+            own_w[w].wait()
         else:
-            weight(i).wait_recv()
-        across_copy(i).start()
-        sibling_copy(i).start()
-
-    def second(i):
-        across_copy(i).wait_recv()
-        second_copy(i).start()
+            weight(i, w).wait_recv()
+        across_copy(i, w).start()
+        sibling_copy(i, w).start()
+
+    def second(i, w):
+        across_copy(i, w).wait_recv()
+        second_copy(i, w).start()
+
+    def settle(w):
+        for i in range(n_sp):
+            source = lax.rem(s - i + n_sp, n_sp)
+            theirs = block(sibling, source, w)
+            remote(theirs, theirs, c_s.at[w, i], c_r.at[w, i], {"tp": sibling}).wait_recv()
+            theirs = block(lax.rem(sibling + 2, n_tp), source, w)
+            remote(theirs, theirs, f_s.at[w, i], f_r.at[w, i], {"tp": sibling}).wait_recv()
 
     query_refs = (q1_ref, q2_ref)
 
@@ -315,21 +328,18 @@
 
     order = [0] + even + odd
     own_kv.wait()
-    relay(order[0])
+    relay(order[0], 0)
     over_in(0).wait_recv()
     attend(0)
-    done, crossed = 1, 0
     for j in range(1, half):
-        relay(order[done])
-        done += 1
 
         @pl.when(z >= j)
         def _(j=j):
             over_in(j).wait_recv()
             attend(j)
 
-        second(order[crossed])
-        crossed += 1
+        relay(order[j], 0)
+        second(order[j - 1], 0)
 
     mixed = acc[0] / low[0] - lam_ref[0, 0] * acc[1] / low[1]
     mean_square = jnp.mean(mixed * mixed, axis=1, keepdims=True)
@@ -360,11 +370,6 @@
         two.start()
         sent += [one, two]
     rbuf[:, here] = res_ref[take(t), :]
-    while done < n_sp - 2:
-        relay(order[done])
-        done += 1
-        second(order[crossed])
-        crossed += 1
     total = part_ref[take(t), :].astype(jnp.float32)
     for copy in sent:
         copy.wait()
@@ -387,44 +392,50 @@
         copy.start()
         z_in.append(copy)
     nall[y, z] = normed
-    while crossed < n_sp:
-        if done < n_sp:
-            relay(order[done])
-            done += 1
-        second(order[crossed])
-        crossed += 1
+    for i in even + odd:
+        weight(i, 1).start()
+    for k in range(half, n_sp):
+        relay(order[k], 0)
+        second(order[k - 1], 0)
+    second(order[n_sp - 1], 0)
     for j in range(1, half):
         z_in[j - 1].wait_recv()
         held = nall.at[y, lax.rem(z - j + half, half)]
         copy = remote(held, held, y_s.at[j], y_r.at[j], {"sp": y_peer})
         copy.start()
         y_in.append(copy)
-    for i in range(n_sp):
-        source = lax.rem(s - i + n_sp, n_sp)
-        theirs = block(sibling, source)
-        remote(theirs, theirs, c_s.at[i], c_r.at[i], {"tp": sibling}).wait_recv()
-        theirs = block(lax.rem(sibling + 2, n_tp), source)
-        remote(theirs, theirs, f_s.at[i], f_r.at[i], {"tp": sibling}).wait_recv()
-
+    settle(0)
     units = n_tp * part
 
-    def mixer(parity, slot):
+    def gated(parity, slot):
         tokens = nall[parity].reshape(half * out_rows, width)
         gate_act = last_dot(tokens, wall[0].reshape(units, width))
         up_act = last_dot(tokens, wall[1].reshape(units, width))
-        hidden = (gate_act / (1.0 + jnp.exp(-gate_act)) * up_act).astype(jnp.bfloat16)
+        hidden[slot] = (gate_act / (1.0 + jnp.exp(-gate_act)) * up_act).astype(jnp.bfloat16)
+
+    def down(slot):
         for k in range(0, width, 512):
             product = jnp.dot(
-                hidden,
+                hidden[slot],
                 wall[2, :, :, k : k + 512].reshape(units, 512),
                 preferred_element_type=jnp.float32,
             ).astype(jnp.bfloat16)
             part2[slot, :, :, k : k + 512] = product.reshape(half, out_rows, 512)
 
-    mixer(y, 0)
+    gated(y, 0)
+    relay(order[0], 1)
+    for k in range(1, half):
+        relay(order[k], 1)
+        second(order[k - 1], 1)
     for copy in y_in:
         copy.wait_recv()
-    mixer(1 - y, 1)
+    gated(1 - y, 1)
+    for k in range(half, n_sp):
+        relay(order[k], 1)
+        second(order[k - 1], 1)
+    second(order[n_sp - 1], 1)
+    settle(1)
+    down(1)
     turn = list(range(1, half)) + [0]
     e_in = {}
     for j in turn:
@@ -432,6 +443,7 @@
         copy = remote(part2.at[1, zi], ybuf.at[j], e_s.at[j], e_r.at[j], {"sp": y_peer})
         copy.start()
         e_in[j] = copy
+    down(0)
     g_in = []
     for j in turn:
         e_in[j].wait_recv()
@@ -467,12 +479,13 @@
         e_in[j].wait_send()
     for copy in o_in:
         copy.wait()
-    for i in range(n_sp):
-        if i > 0:
-            weight(i).wait_send()
-        across_copy(i).wait_send()
-        sibling_copy(i).wait_send()
-        second_copy(i).wait_send()
+    for w in range(2):
+        for i in range(n_sp):
+            if i > 0:
+                weight(i, w).wait_send()
+            across_copy(i, w).wait_send()
+            sibling_copy(i, w).wait_send()
+            second_copy(i, w).wait_send()
     over(0).wait_send()
 
     @pl.when(z < half - 1)
@@ -509,6 +522,7 @@
             pltpu.VMEM((three, n_tp, ff_here // n_sp, depth * n_sp), bf16),
             pltpu.VMEM(rowblock, bf16),
             pltpu.VMEM((2, half) + rowblock, bf16),
+            pltpu.VMEM((2, half * rows, n_tp * (ff_here // n_sp)), bf16),
             pltpu.VMEM((2, half) + rowblock, bf16),
             pltpu.VMEM((half,) + rowblock, bf16),
             pltpu.VMEM((half - 1,) + rowblock, bf16),
@@ -524,9 +538,9 @@
             pltpu.VMEM(rowblock, bf16),
         ]
         + [dma((half,))] * 4
-        + [dma((n_sp - 1,))] * 2
-        + [dma((n_sp,))] * 6
-        + [dma((2,))]
+        + [dma((2, n_sp - 1))] * 2
+        + [dma((2, n_sp))] * 6
+        + [dma((3,))]
         + [dma((n_tp - 1,))] * 4
         + [dma((half - 1,))] * 2
         + [dma((half,))] * 4

time: 158 us -> 165 us (1.044)
  Pallas kernels: 149 us -> 157 us
    pallas_call x1, Pallas kernels: 149 us -> 157 us  [front(): pl.pallas_call(functools.partial(front_kernel, n_sp, n_tp), out_shape=jax...]
where the time goes in v4:
time: 165 us; the launch traced here: 164 us
  Pallas kernels  157 us (95%)
  local copies, waits for them, and re-layouts  4.52 us (3%)
  other arithmetic  2.33 us (1%)
    pallas_call x1, Pallas kernels, front(): pl.pallas_call(functools.partial(front_kernel, n_sp, n_tp), out_shape=jax...  157 us
    unnamed x11, local copies, waits for them, and re-layouts  4.52 us

profile of v4, /device:TPU:13, one launch (start us, length us, event | category | flops | bytes accessed | tf_op | source)
XLA Modules:
  0.0 164.2 jit_solution(9028513602526934284)
XLA Ops:
  0.0 0.0 copy-start
  0.0 1.4 copy.14
  1.5 1.4 copy.15
  2.8 0.0 copy-done
  2.9 0.0 copy-start.1
  2.9 0.0 copy-start.2
  2.9 0.0 copy-start.3
  2.9 1.6 pad_maximum_fusion.w_ref
  4.5 0.0 copy-done.1
  4.5 0.0 copy-done.2
  4.5 0.0 copy-done.3
  4.5 0.7 pad_maximum_fusion.1.kv_ref
  5.9 156.6 %front.1 = bf16[256,512]{1,0:T(8,128)(2,1)} custom-call(bf16[3,1408,256]{2,1,0:T(8,128)(2,1)} %pad_maximum_fusion.w_ref, bf16[256,512]{1,0:T(8,128)(2,1)} %pad_maximum_fusion.1.kv_ref, bf16[256,128]{1,0:T(8,128)(2,1)} %q1_ref.1, bf16[256,128]{1,0:T(8,128)(2,1)} %q2_ref.1, f32[1,1]{1,0:T(1,128)} %bitcast.10.lam_ref, f32[1,256]{1,0:T(1,128)} %bitcast.15, ...), custom_call_target="tpu_custom_call" | custom-call | tf_op jit(solution)/shard_map/front/pallas_call | solution.py:516
  162.5 1.7 %copy.18 = bf16[256,512]{1,0:T(8,128)(2,1)} copy(bf16[256,512]{1,0:T(8,128)(2,1)} %front.1) | data formatting | bytes 524288
Async XLA Ops:
  0.0 2.8 %copy-start = (bf16[1408,256]{1,0:T(8,128)(2,1)S(1)}, bf16[1408,256]{1,0:T(8,128)(2,1)}, u32[]{:S(2)}) copy-start(bf16[1408,256]{1,0:T(8,128)(2,1)} %param.25) | copy-start | bytes 2162692
  2.9 1.6 %copy-start.1 = (bf16[256,256]{1,0:T(8,128)(2,1)S(1)}, bf16[256,256]{1,0:T(8,128)(2,1)}, u32[]{:S(2)}) copy-start(bf16[256,256]{1,0:T(8,128)(2,1)} %param.17) | copy-start | bytes 393220
  2.9 1.6 copy-start.2
  2.9 1.6 copy-start.3

commit v5 on v3

--- a/solution.py
+++ b/solution.py
@@ -320,14 +320,14 @@
     attend(0)
     done, crossed = 1, 0
     for j in range(1, half):
-        relay(order[done])
-        done += 1
 
         @pl.when(z >= j)
         def _(j=j):
             over_in(j).wait_recv()
             attend(j)
 
+        relay(order[done])
+        done += 1
         second(order[crossed])
         crossed += 1
 
@@ -360,11 +360,6 @@
         two.start()
         sent += [one, two]
     rbuf[:, here] = res_ref[take(t), :]
-    while done < n_sp - 2:
-        relay(order[done])
-        done += 1
-        second(order[crossed])
-        crossed += 1
     total = part_ref[take(t), :].astype(jnp.float32)
     for copy in sent:
         copy.wait()

time: 158 us -> 167 us (1.057)
  Pallas kernels: 149 us -> 159 us
    pallas_call x1, Pallas kernels: 149 us -> 159 us  [front(): pl.pallas_call(functools.partial(front_kernel, n_sp, n_tp), out_shape=jax...]
where the time goes in v5:
time: 167 us
  Pallas kernels  159 us (95%)
  local copies, waits for them, and re-layouts  4.52 us (3%)
  other arithmetic  2.33 us (1%)
    pallas_call x1, Pallas kernels, front(): pl.pallas_call(functools.partial(front_kernel, n_sp, n_tp), out_shape=jax...  159 us
    unnamed x11, local copies, waits for them, and re-layouts  4.52 us

profile of v5, /device:TPU:13, one launch (start us, length us, event | category | flops | bytes accessed | tf_op | source)
XLA Modules:
  0.0 166.9 jit_solution(4485245203422617116)
XLA Ops:
  0.0 0.0 copy-start
  0.0 1.4 copy.14
  1.5 1.4 copy.15
  2.8 0.0 copy-done
  2.9 0.0 copy-start.1
  2.9 0.0 copy-start.2
  2.9 0.0 copy-start.3
  2.9 1.6 pad_maximum_fusion.w_ref
  4.5 0.0 copy-done.1
  4.5 0.0 copy-done.2
  4.5 0.0 copy-done.3
  4.5 0.7 pad_maximum_fusion.1.kv_ref
  5.9 159.4 %front.1 = bf16[256,512]{1,0:T(8,128)(2,1)} custom-call(bf16[3,1408,256]{2,1,0:T(8,128)(2,1)} %pad_maximum_fusion.w_ref, bf16[256,512]{1,0:T(8,128)(2,1)} %pad_maximum_fusion.1.kv_ref, bf16[256,128]{1,0:T(8,128)(2,1)} %q1_ref.1, bf16[256,128]{1,0:T(8,128)(2,1)} %q2_ref.1, f32[1,1]{1,0:T(1,128)} %bitcast.10.lam_ref, f32[1,256]{1,0:T(1,128)} %bitcast.15, ...), custom_call_target="tpu_custom_call" | custom-call | tf_op jit(solution)/shard_map/front/pallas_call | solution.py:498
  165.3 1.7 %copy.18 = bf16[256,512]{1,0:T(8,128)(2,1)} copy(bf16[256,512]{1,0:T(8,128)(2,1)} %front.1) | data formatting | bytes 524288
Async XLA Ops:
  0.0 2.8 %copy-start = (bf16[1408,256]{1,0:T(8,128)(2,1)S(1)}, bf16[1408,256]{1,0:T(8,128)(2,1)}, u32[]{:S(2)}) copy-start(bf16[1408,256]{1,0:T(8,128)(2,1)} %param.25) | copy-start | bytes 2162692
  2.9 1.6 copy-start.1
  2.9 1.6 copy-start.2
  2.9 1.6 copy-start.3
